TPU v7x, 32 devices: a whole 2x2x4 slice. The times are simulated.
32 devices in a mesh: sp: 4 (over y, x), dp: 8 (over z, core).
Axes of the slice: x: 2, y: 2, z: 4, core: 2. Of those that a mesh axis runs over, the one named last changes fastest.
Arguments:
- value_half: bfloat16 [8, 1024, 2048], P('dp', 'sp'), may hold values from -6 to 6
- gate_half: bfloat16 [8, 1024, 2048], P('dp', 'sp'), may hold values from -6 to 6
- upstream: bfloat16 [8, 1024, 2048], P('dp', 'sp'), may hold values from -6 to 6
- conv_taps: float32 [31, 2048], P(None, 'sp'), may hold values from -1 to 1
- norm_gain: float32 [2048], replicated, may hold values from 0.1 to 1.9
- out_weight: bfloat16 [2048, 2048], P('dp'), may hold values from -0.125 to 0.125
Outputs:
- grad_value: bfloat16 [8, 1024, 2048], P('dp', 'sp')
- grad_gate: bfloat16 [8, 1024, 2048], P('dp', 'sp')
- grad_taps: float32 [31, 2048], P(None, 'sp')
- grad_gain: float32 [2048], replicated
- grad_weight: float32 [2048, 2048], P('dp')
All inputs are finite; a program needn't handle non-finite values.
Results may differ from a plain program's by a relative error of at most 0.0062.
Values may be sent and summed in bfloat16 or wider, within the bound.
A program may use at most 128 MiB of HBM per device.

v0:
```python
import jax
import jax.numpy as jnp
from jax import lax
from jax.sharding import PartitionSpec as P

NORM_EPS = 1e-05


def body(value_half, gate_half, upstream, conv_taps, norm_gain, out_weight):
    tap_count = conv_taps.shape[0]
    sig_gate = jax.nn.sigmoid(gate_half.astype(jnp.float32))
    value_wide = value_half.astype(jnp.float32)
    glu = (value_wide * sig_gate).astype(jnp.bfloat16)
    glu_heads = lax.all_to_all(glu, "sp", split_axis=2, concat_axis=1, tiled=True).astype(
        jnp.float32
    )
    length = glu_heads.shape[1]
    padded = jnp.pad(glu_heads, ((0, 0), (tap_count - 1, 0), (0, 0)))
    conv_out = jnp.zeros_like(glu_heads)
    for offset in range(tap_count):
        conv_out = conv_out + conv_taps[offset] * padded[:, offset : offset + length]
    conv_tokens = lax.all_to_all(
        conv_out.astype(jnp.bfloat16), "sp", split_axis=1, concat_axis=2, tiled=True
    ).astype(jnp.float32)
    row_mean = jnp.mean(conv_tokens, axis=-1, keepdims=True)
    centered = conv_tokens - row_mean
    inv_scale = lax.rsqrt(jnp.mean(centered * centered, axis=-1, keepdims=True) + NORM_EPS)
    normed = centered * inv_scale
    scaled = normed * norm_gain
    sig_scaled = jax.nn.sigmoid(scaled)
    activated = (scaled * sig_scaled).astype(jnp.bfloat16)[0]
    upstream_rows = upstream[0]
    columns = upstream_rows
    grad_act = jnp.dot(
        columns,
        lax.all_gather(out_weight, "dp", axis=0, tiled=True),
        preferred_element_type=jnp.float32,
    )
    grad_scaled = grad_act[None] * sig_scaled * (1.0 + scaled * (1.0 - sig_scaled))
    gain_part = jnp.sum(grad_scaled * normed, axis=(0, 1))
    grad_normed = grad_scaled * norm_gain
    grad_conv_out = inv_scale * (
        grad_normed
        - jnp.mean(grad_normed, axis=-1, keepdims=True)
        - normed * jnp.mean(grad_normed * normed, axis=-1, keepdims=True)
    )
    grad_heads = lax.all_to_all(
        grad_conv_out.astype(jnp.bfloat16), "sp", split_axis=2, concat_axis=1, tiled=True
    ).astype(jnp.float32)
    grad_padded = jnp.pad(grad_heads, ((0, 0), (0, tap_count - 1), (0, 0)))
    grad_glu = jnp.zeros_like(grad_heads)
    tap_terms = []
    for offset in range(tap_count):
        first = tap_count - 1 - offset
        grad_glu = grad_glu + conv_taps[offset] * grad_padded[:, first : first + length]
        tap_terms.append(jnp.sum(grad_heads * padded[:, offset : offset + length], axis=(0, 1)))
    grad_taps = lax.psum(jnp.stack(tap_terms), "dp")
    grad_tokens = lax.all_to_all(
        grad_glu.astype(jnp.bfloat16), "sp", split_axis=1, concat_axis=2, tiled=True
    ).astype(jnp.float32)
    grad_value = (grad_tokens * sig_gate).astype(jnp.bfloat16)
    grad_gate = (grad_tokens * value_wide * sig_gate * (1.0 - sig_gate)).astype(jnp.bfloat16)
    grad_gain = lax.psum(gain_part, ("sp", "dp"))
    columns = upstream_rows
    owned = lax.psum_scatter(
        lax.dot_general(
            columns, activated, (((0,), (0,)), ((), ())), preferred_element_type=jnp.float32
        ),
        "dp",
        scatter_dimension=0,
        tiled=True,
    )
    grad_weight = lax.psum(owned, "sp")
    return (grad_value, grad_gate, grad_taps, grad_gain, grad_weight)


def solution(mesh):
    placed = (
        P("dp", "sp", None),
        P("dp", "sp", None),
        P("dp", "sp", None),
        P(None, "sp"),
        P(),
        P("dp", None),
    )
    return jax.shard_map(
        body,
        mesh=mesh,
        in_specs=placed,
        out_specs=(P("dp", "sp", None), P("dp", "sp", None), P(None, "sp"), P(), P("dp", None)),
        check_vma=False,
    )
```

profile of v0, /device:TPU:0, one launch (start us, length us, event | category | flops | bytes accessed | tf_op | source)
XLA Modules:
  0.0 395.5 jit_solution(13518251392995277205)
XLA Ops:
  7.9 1.5 copy.56
  9.4 1.9 copy.57
  11.9 12.9 %copy.90 = bf16[1,256,2048]{1,0,2:T(2,128)(2,1)} copy(bf16[1,256,2048]{1,2,0:T(8,128)(2,1)S(1)} %fusion.1) | data formatting | bytes 2097152 | tf_op jit(solution)/shard_map/convert_element_type | solution.py:13
  25.3 11.6 %reduce.17 = bf16[2048,256]{1,0:T(8,128)(2,1)S(1)} reduce(bf16[2048,1,256]{2,1,0:T(2,128)(2,1)} %bitcast.178, bf16[]{:T(256)} %broadcast.201), dimensions={1}, to_apply=%bitcast.161.reduce_sub_computation | reduce | bytes 2097154
  37.0 1.6 reshape.389
  38.6 5.4 %all-to-all-start = ((bf16[4,2,65536]{2,1,0:T(2,128)(2,1)}), bf16[4,2,65536]{2,1,0:T(2,128)(2,1)}, u32[]{:S(2)}, u32[]{:S(2)}) async-start(bf16[4,2,65536]{2,1,0:T(2,128)(2,1)} %reshape.389), calls=%async_computation | async-start | bytes 2097152 | tf_op jit(solution)/shard_map/all_to_all | solution.py:14
  44.1 14.2 %all-to-all-done = bf16[4,2,65536]{2,1,0:T(2,128)(2,1)} async-done(((bf16[4,2,65536]{2,1,0:T(2,128)(2,1)}), bf16[4,2,65536]{2,1,0:T(2,128)(2,1)}, u32[]{:S(2)}, u32[]{:S(2)}) %all-to-all-start) | async-done | bytes 1048608 | tf_op jit(solution)/shard_map/all_to_all | solution.py:14
  58.3 2.6 reshape.390
  60.9 1.6 copy_convert_fusion.2
  63.0 1.9 copy.60
  64.9 8.0 %add_convert_fusion.1 = bf16[1,1024,512]{2,1,0:T(8,128)(2,1)S(1)} fusion(f32[1,1024,512]{2,1,0:T(8,128)S(1)} %bitcast.163, f32[512]{0:T(512)S(1)} %bitcast.207, f32[512]{0:T(512)S(1)} %bitcast.209, f32[512]{0:T(512)S(1)} %bitcast.213, f32[512]{0:T(512)S(1)} %bitcast.215, f32[512]{0:T(512)S(1)} %bitcast.217, f32[512]{0:T(512)S(1)} %bitcast.219, ...), kind=kLoop, calls=%fused_computation.88 | loop fusion | flops 32505856 | bytes 3209216 | tf_op jit(solution)/shard_map/convert_element_type | solution.py:23
  72.9 2.9 copy.89
  75.8 8.1 %reduce.18 = bf16[1024,512]{1,0:T(8,128)(2,1)S(1)} reduce(bf16[1024,1,512]{2,1,0:T(2,128)(2,1)} %bitcast.180, bf16[]{:T(256)} %broadcast.201), dimensions={1}, to_apply=%bitcast.160.reduce_sub_computation | reduce | bytes 2097154
  83.9 2.0 reshape.391
  85.9 4.3 %all-to-all-start.1 = ((bf16[4,2,65536]{2,1,0:T(2,128)(2,1)}), bf16[4,2,65536]{2,1,0:T(2,128)(2,1)}, u32[]{:S(2)}, u32[]{:S(2)}) async-start(bf16[4,2,65536]{2,1,0:T(2,128)(2,1)} %reshape.391), calls=%async_computation.1 | async-start | bytes 2097152 | tf_op jit(solution)/shard_map/all_to_all | solution.py:22
  90.2 13.4 %all-to-all-done.1 = bf16[4,2,65536]{2,1,0:T(2,128)(2,1)} async-done(((bf16[4,2,65536]{2,1,0:T(2,128)(2,1)}), bf16[4,2,65536]{2,1,0:T(2,128)(2,1)}, u32[]{:S(2)}, u32[]{:S(2)}) %all-to-all-start.1) | async-done | bytes 1048608 | tf_op jit(solution)/shard_map/all_to_all | solution.py:22
  103.6 3.0 reshape.392
  108.0 1.8 copy_convert_fusion.1
  109.8 1.8 copy.63
  111.6 1.9 fusion.10
  113.5 1.8 fusion.32
  115.4 2.3 copy.71
  117.6 9.3 %convolution_bitcast_fusion = f32[2048,2048]{0,1:T(8,128)} fusion(bf16[256,2048]{0,1:T(8,128)(2,1)} %bitcast.186, bf16[1,256,2048]{2,1,0:T(8,128)(2,1)S(1)} %copy-done), kind=kOutput, calls=%fused_computation | convolution fusion | flops 2147483648 | bytes 18874368 | tf_op jit(solution)/shard_map/dot_general | solution.py:66
  126.9 1.4 copy.64
  129.2 5.7 %multiply_reduce_fusion = (f32[2048]{0:T(1024)S(1)}, f32[256]{0:T(256)S(1)}, f32[256]{0:T(256)S(1)}, f32[256,2048]{1,0:T(8,128)S(1)}) fusion(f32[256,2048]{1,0:T(8,128)S(1)} %bitcast.176, f32[256]{0:T(256)S(1)} %broadcast_multiply_fusion.2, f32[256]{0:T(256)S(1)} %add_rsqrt_fusion, f32[2048]{0:T(1024)S(1)} %copy-done.11, ...), kind=kOutput, calls=%fused_computation.20 | convolution fusion | flops 2156393984 | bytes 13651968 | tf_op jit(solution)/shard_map/dot_general | solution.py:34
  135.7 1.7 copy.65
  137.4 10.8 %reduce.19 = bf16[2048,256]{1,0:T(8,128)(2,1)S(1)} reduce(bf16[2048,1,256]{2,1,0:T(2,128)(2,1)S(1)} %bitcast.182, bf16[]{:T(256)} %broadcast.201), dimensions={1}, to_apply=%bitcast.148.reduce_sub_computation | reduce | bytes 2097154
  148.1 1.6 reshape.393
  149.8 3.5 all-to-all-start.2
  153.4 48.8 %psum.22 = f32[2048]{0:T(1024)} all-reduce(f32[2048]{0:T(1024)S(1)} %get-tuple-element.35), channel_id=1, replica_groups=mesh['sp'=4,'dp'=8] {'sp','dp'}, use_global_device_ids=true, to_apply=%region_39.40 | all-reduce | flops 2048 | bytes 16384 | tf_op jit(solution)/shard_map/psum | solution.py:63
  203.1 1.6 copy_convert_fusion
  205.1 1.9 copy.67
  207.1 8.0 %add_convert_fusion = bf16[1,1024,512]{2,1,0:T(8,128)(2,1)S(1)} fusion(f32[1,1024,512]{2,1,0:T(8,128)S(1)} %bitcast.162, f32[512]{0:T(512)S(1)} %bitcast.208, f32[512]{0:T(512)S(1)} %bitcast.210, f32[512]{0:T(512)S(1)} %bitcast.214, f32[512]{0:T(512)S(1)} %bitcast.216, f32[512]{0:T(512)S(1)} %bitcast.218, f32[512]{0:T(512)S(1)} %bitcast.220, ...), kind=kLoop, calls=%fused_computation.52 | loop fusion | flops 32505856 | bytes 3209216 | tf_op jit(solution)/shard_map/convert_element_type | solution.py:59
  215.0 81.4 %reduce-scatter.2.cloned.1.call-done = f32[256,2048]{0,1:T(8,128)} async-done(((f32[2048,2048]{0,1:T(8,128)}), f32[256,2048]{0,1:T(8,128)}) %reduce-scatter.2.cloned.1.call-update) | async-done | bytes 2097168 | tf_op jit(solution)/shard_map/reduce_scatter | solution.py:65
  296.5 17.9 %multiply_reduce_fusion.2 = (f32[512]{0:T(512)S(1)}, f32[512]{0:T(512)S(1)}, f32[512]{0:T(512)S(1)}, f32[512]{0:T(512)S(1)}, f32[512]{0:T(512)S(1)}, /*index=5*/...) fusion(f32[1,1024,512]{2,1,0:T(8,128)} %bitcast.164, ...), kind=kLoop, calls=%fused_computation.22 | loop fusion | flops 18865152 | bytes 4231168 | tf_op jit(solution)/shard_map/reduce_sum | solution.py:56
  314.4 2.9 copy.88
  317.4 8.0 %reduce.20 = bf16[1024,512]{1,0:T(8,128)(2,1)S(1)} reduce(bf16[1024,1,512]{2,1,0:T(2,128)(2,1)} %bitcast.179, bf16[]{:T(256)} %broadcast.201), dimensions={1}, to_apply=%bitcast.159.reduce_sub_computation | reduce | bytes 2097154
  325.4 2.0 reshape.395
  327.4 3.7 all-to-all-start.3
  331.1 2.6 multiply_reduce_fusion.1
  333.7 11.8 %multiply_reduce_fusion.3 = (f32[512]{0:T(512)S(1)}, f32[512]{0:T(512)S(1)}, f32[512]{0:T(512)S(1)}, f32[512]{0:T(512)S(1)}, f32[512]{0:T(512)S(1)}, /*index=5*/...) fusion(f32[1,1024,512]{2,1,0:T(8,128)} %bitcast.165, ...), kind=kLoop, calls=%fused_computation.23 | loop fusion | flops 12576768 | bytes 4218880 | tf_op jit(solution)/shard_map/reduce_sum | solution.py:56
  345.7 27.2 %psum.21 = f32[31,512]{1,0:T(8,128)} all-reduce(f32[31,512]{1,0:T(8,128)S(1)} %stack.127), channel_id=1, replica_groups=mesh['sp'=4,'dp'=8] {'dp'}, use_global_device_ids=true, to_apply=%region_37.38 | all-reduce | flops 15872 | bytes 126976 | tf_op jit(solution)/shard_map/psum | solution.py:57
  374.1 1.6 convert_bitcast_fusion
  375.7 3.0 copy.70
  378.8 3.4 fusion.4
  382.1 2.3 copy.72
  384.4 1.4 copy.73
  385.8 2.9 copy.74
  (53 shorter events, 8.3 us)
Async XLA Ops:
  7.2 110.5 %copy-start = (bf16[1,256,2048]{2,1,0:T(8,128)(2,1)S(1)}, bf16[1,256,2048]{2,1,0:T(8,128)(2,1)}, u32[]{:S(2)}) copy-start(bf16[1,256,2048]{2,1,0:T(8,128)(2,1)} %param.8) | copy-start | bytes 3145732
  7.2 122.0 %all-gather.2.cloned.1.call-start = ((), (), s32[]{:S(2)}) async-start(), calls=%async_computation.5 | async-start | bytes 9437184 | tf_op jit(solution)/shard_map/all_gather | solution.py:36
  9.4 2.5 copy-start.6
  11.3 13.5 %copy-start.8 = (bf16[1,256,2048]{1,2,0:T(8,128)(2,1)}, bf16[1,256,2048]{1,2,0:T(8,128)(2,1)S(1)}, u32[]{:S(2)}) copy-start(bf16[1,256,2048]{1,2,0:T(8,128)(2,1)S(1)} %copy.57) | copy-start | bytes 3145732
  37.0 7.1 %copy-start.10 = (f32[31,512]{1,0:T(8,128)S(1)}, f32[31,512]{1,0:T(8,128)}, u32[]{:S(2)}) copy-start(f32[31,512]{1,0:T(8,128)} %param.9) | copy-start | bytes 190468
  38.6 19.7 %all-to-all-start = ((bf16[4,2,65536]{2,1,0:T(2,128)(2,1)}), bf16[4,2,65536]{2,1,0:T(2,128)(2,1)}, u32[]{:S(2)}, u32[]{:S(2)}) async-start(bf16[4,2,65536]{2,1,0:T(2,128)(2,1)} %reshape.389), calls=%async_computation | async-start | bytes 2097152 | tf_op jit(solution)/shard_map/all_to_all | solution.py:14
  60.9 2.0 copy-start.3
  64.9 10.9 %copy-start.2 = (f32[1,4,256,512]{3,2,1,0:T(8,128)}, f32[1,4,256,512]{3,2,1,0:T(8,128)S(1)}, u32[]{:S(2)}) copy-start(f32[1,4,256,512]{3,2,1,0:T(8,128)S(1)} %copy.60) | copy-start | bytes 6291460
  83.9 6.3 %copy-start.11 = (f32[2048]{0:T(1024)S(1)}, f32[2048]{0:T(1024)}, u32[]{:S(2)}) copy-start(f32[2048]{0:T(1024)} %param.10) | copy-start | bytes 24580
  85.9 17.7 %all-to-all-start.1 = ((bf16[4,2,65536]{2,1,0:T(2,128)(2,1)}), bf16[4,2,65536]{2,1,0:T(2,128)(2,1)}, u32[]{:S(2)}, u32[]{:S(2)}) async-start(bf16[4,2,65536]{2,1,0:T(2,128)(2,1)} %reshape.391), calls=%async_computation.1 | async-start | bytes 2097152 | tf_op jit(solution)/shard_map/all_to_all | solution.py:22
  90.2 206.3 %reduce-scatter.2.cloned.1.call-start = ((), (), s32[]{:S(2)}) async-start(), calls=%async_computation.6 | async-start | bytes 18874368 | tf_op jit(solution)/shard_map/reduce_scatter | solution.py:65
  106.6 1.3 copy-start.5
  149.8 52.3 %all-to-all-start.2 = ((bf16[4,2,65536]{2,1,0:T(2,128)(2,1)}), bf16[4,2,65536]{2,1,0:T(2,128)(2,1)S(1)}, u32[]{:S(2)}, u32[]{:S(2)}) async-start(bf16[4,2,65536]{2,1,0:T(2,128)(2,1)} %reshape.393), calls=%async_computation.2 | async-start | bytes 2097152 | tf_op jit(solution)/shard_map/all_to_all | solution.py:47
  153.3 232.5 %all-reduce.4.cloned.1.call-start = ((), (), s32[]{:S(2)}) async-start(), calls=%async_computation.7 | async-start | bytes 4194304 | tf_op jit(solution)/shard_map/psum | solution.py:73
  203.1 2.0 copy-start.4
  327.4 45.5 %all-to-all-start.3 = ((bf16[4,2,65536]{2,1,0:T(2,128)(2,1)}), bf16[4,2,65536]{2,1,0:T(2,128)(2,1)S(1)}, u32[]{:S(2)}, u32[]{:S(2)}) async-start(bf16[4,2,65536]{2,1,0:T(2,128)(2,1)} %reshape.395), calls=%async_computation.3 | async-start | bytes 2097152 | tf_op jit(solution)/shard_map/all_to_all | solution.py:58
  375.7 3.0 copy-start.7
  375.7 3.0 copy-start.9
  384.4 4.3 %copy-start.1 = (bf16[1,256,2048]{2,1,0:T(8,128)(2,1)S(1)}, bf16[1,256,2048]{2,1,0:T(8,128)(2,1)}, u32[]{:S(2)}) copy-start(bf16[1,256,2048]{2,1,0:T(8,128)(2,1)} %param.8) | copy-start | bytes 3145732
Sparse Core Ops, SparseCore 0:
  9.6 84.7 all-gather.1
  127.1 169.3 reduce-scatter.1
  299.6 69.1 all-reduce.3
where the time goes:
time: 402 us; the launch traced here: 395 us
  waiting for transfers between devices  110 us (27%)
  other arithmetic  102 us (25%)
  blocking collectives  75.9 us (19%)
  local copies, waits for them, and re-layouts  61.5 us (15%)
  starting transfers between devices  16.9 us (4%)
  matrix products  15 us (4%)
  between operations  14.3 us (4%)
    reduce_scatter x1, waiting for transfers between devices, body(): lax.psum_scatter(lax.dot_general(columns, activated, (((0,), (0,)), ((),...  81.4 us
    psum x1, blocking collectives, body(): grad_gain = lax.psum(gain_part, ('sp', 'dp'))  48.8 us
    unnamed x4, other arithmetic  38.5 us
    reduce_sum x4, other arithmetic, body(): jnp.sum(grad_heads * padded[:, offset:offset + length], axis=(0, 1))  32.4 us
    unnamed x39, local copies, waits for them, and re-layouts  28.2 us
    psum x1, blocking collectives, body(): grad_taps = lax.psum(jnp.stack(tap_terms), 'dp')  27.2 us
    all_to_all x1, waiting for transfers between devices, body(): lax.all_to_all(glu, 'sp', split_axis=2, concat_axis=1, tiled=True)  14.2 us
    all_to_all x1, waiting for transfers between devices, body(): lax.all_to_all(conv_out.astype(jnp.bfloat16), 'sp', split_axis=1, concat_...  13.4 us
  transfers between devices with their start and end apart: 7, of which 3 were waited for; matrix products, arithmetic and copies ran while one was open for 44% of the time, Pallas kernels for 0%

commit v1 on v0

v1 whole, which is shorter than its diff:
```python
import jax
import jax.numpy as jnp
from jax import lax
from jax.sharding import PartitionSpec as P

NORM_EPS = 1e-05


def body(value_half, gate_half, upstream, conv_taps, norm_gain, out_weight):
    f32 = jnp.float32
    tap_count = conv_taps.shape[0]
    halo = tap_count - 1
    sp = lax.axis_size("sp")
    onward = [(i, i + 1) for i in range(sp - 1)]
    back = [(i + 1, i) for i in range(sp - 1)]

    value = value_half[0].astype(f32)
    gate = gate_half[0].astype(f32)
    length = value.shape[0]
    weight = lax.all_gather(out_weight, "dp", axis=0, tiled=True)
    up = upstream[0]
    up_columns = lax.all_to_all(up, "dp", split_axis=1, concat_axis=0, tiled=True)
    taps = lax.all_gather(conv_taps, "sp", axis=1, tiled=True)

    tail = (value[length - halo :] * jax.nn.sigmoid(gate[length - halo :])).astype(jnp.bfloat16)
    before = lax.ppermute(tail, "sp", onward)
    sig_gate = jax.nn.sigmoid(gate)
    glu = (value * sig_gate).astype(jnp.bfloat16)
    padded = jnp.concatenate([before, glu], axis=0).astype(f32)
    conv = jnp.zeros((length, padded.shape[1]), f32)
    for j in range(tap_count):
        conv = conv + taps[j] * padded[j : j + length]
    conv = conv.astype(jnp.bfloat16).astype(f32)
    mean = jnp.mean(conv, axis=-1, keepdims=True)
    centered = conv - mean
    inv = lax.rsqrt(jnp.mean(centered * centered, axis=-1, keepdims=True) + NORM_EPS)
    normed = centered * inv
    scaled = normed * norm_gain
    sig = jax.nn.sigmoid(scaled)
    activated = (scaled * sig).astype(jnp.bfloat16)
    act_all = lax.all_gather(activated, "dp", axis=0, tiled=True)

    grad_act = jnp.dot(up, weight, preferred_element_type=f32)
    grad_scaled = grad_act * sig * (1.0 + scaled * (1.0 - sig))
    gain_part = jnp.sum(grad_scaled * normed, axis=0)
    g = grad_scaled * norm_gain
    grad_conv = inv * (
        g
        - jnp.mean(g, axis=-1, keepdims=True)
        - normed * jnp.mean(g * normed, axis=-1, keepdims=True)
    )
    grad_conv = grad_conv.astype(jnp.bfloat16)
    after = lax.ppermute(grad_conv[:halo], "sp", back)
    extended = jnp.concatenate([grad_conv, after], axis=0).astype(f32)
    here = grad_conv.astype(f32)
    grad_glu = jnp.zeros_like(here)
    terms = []
    for j in range(tap_count):
        first = halo - j
        grad_glu = grad_glu + taps[j] * extended[first : first + length]
        terms.append(jnp.sum(here * padded[j : j + length], axis=0))
    sums = lax.psum(jnp.stack(terms + [gain_part]), ("sp", "dp"))
    width = conv_taps.shape[1]
    grad_taps = lax.dynamic_slice_in_dim(
        sums[:tap_count], lax.axis_index("sp") * width, width, axis=1
    )
    grad_gain = sums[tap_count]
    grad_glu = grad_glu.astype(jnp.bfloat16).astype(f32)
    grad_value = (grad_glu * sig_gate).astype(jnp.bfloat16)
    grad_gate = (grad_glu * value * sig_gate * (1.0 - sig_gate)).astype(jnp.bfloat16)

    owned = lax.dot_general(
        up_columns, act_all, (((0,), (0,)), ((), ())), preferred_element_type=f32
    )
    grad_weight = lax.psum(owned, "sp")
    return (grad_value[None], grad_gate[None], grad_taps, grad_gain, grad_weight)


def solution(mesh):
    tokens = P("dp", "sp", None)
    return jax.shard_map(
        body,
        mesh=mesh,
        in_specs=(tokens, tokens, tokens, P(None, "sp"), P(), P("dp", None)),
        out_specs=(tokens, tokens, P(None, "sp"), P(), P("dp", None)),
        check_vma=False,
    )
```

time: 402 us -> 419 us (1.042); the launches traced: 395 us -> 419 us
  waiting for transfers between devices: 110 us -> 308 us
  blocking collectives: 75.9 us -> 9.08 us
  other arithmetic: 102 us -> 39.9 us
  local copies, waits for them, and re-layouts: 61.5 us -> 19.3 us
  starting transfers between devices: 16.9 us -> 10.9 us
    psum x0 -> x1, waiting for transfers between devices: none -> 110 us  [body(): sums = lax.psum(jnp.stack(terms + [gain_part]), ('sp', 'dp'))]
    reduce_scatter x1 -> x0, waiting for transfers between devices: 81.4 us -> none  [body(): lax.psum_scatter(lax.dot_general(columns, activated, (((0,), (0,)), ((),...]
    psum x2 -> x0, blocking collectives: 75.9 us -> none  [the longest x1 48.8 us: body(): grad_gain = lax.psum(gain_part, ('sp', 'dp'))]
    all_gather x1 -> x2, waiting for transfers between devices: 0.02 us -> 73.1 us  [the longest x1 56.8 us: body(): weight = lax.all_gather(out_weight, 'dp', axis=0, tiled=True)]
    psum x1, waiting for transfers between devices: 0.01 us -> 69.2 us  [body(): grad_weight = lax.psum(owned, 'sp')]
    unnamed x4 -> x0, other arithmetic: 38.5 us -> none
    convert_element_type x10 -> x0, local copies, waits for them, and re-layouts: 32.8 us -> none  [the longest x1 12.9 us: body(): glu = (value_wide * sig_gate).astype(jnp.bfloat16)]
    all_to_all x4 -> x1, waiting for transfers between devices: 27.6 us -> 54.7 us  [body(): lax.all_to_all(up, 'dp', split_axis=1, concat_axis=0, tiled=True)]
  transfers between devices with their start and end apart: 7 -> 7, of which waited for: 3 -> 5; matrix products, arithmetic and copies ran while one was open for 44% -> 15% of each run, Pallas kernels for 0% -> 0%
where the time goes in v1:
time: 419 us
  waiting for transfers between devices  308 us (74%)
  other arithmetic  39.9 us (10%)
  local copies, waits for them, and re-layouts  19.3 us (5%)
  matrix products  16.9 us (4%)
  between operations  14.5 us (3%)
  starting transfers between devices  10.9 us (3%)
  blocking collectives  9.08 us (2%)
    psum x1, waiting for transfers between devices, body(): sums = lax.psum(jnp.stack(terms + [gain_part]), ('sp', 'dp'))  110 us
    psum x1, waiting for transfers between devices, body(): grad_weight = lax.psum(owned, 'sp')  69.2 us
    all_gather x1, waiting for transfers between devices, body(): weight = lax.all_gather(out_weight, 'dp', axis=0, tiled=True)  56.8 us
    all_to_all x1, waiting for transfers between devices, body(): lax.all_to_all(up, 'dp', split_axis=1, concat_axis=0, tiled=True)  54.7 us
    all_gather x1, waiting for transfers between devices, body(): act_all = lax.all_gather(activated, 'dp', axis=0, tiled=True)  16.3 us
    reduce_sum x2, other arithmetic, body(): terms.append(jnp.sum(here * padded[j:j + length], axis=0))  12.5 us
    reduce_sum x1, other arithmetic, body(): mean = jnp.mean(conv, axis=-1, keepdims=True)  10.7 us
    broadcast_in_dim x1, other arithmetic, body(): grad_gate[None]  10.6 us
  transfers between devices with their start and end apart: 7, of which 5 were waited for; matrix products, arithmetic and copies ran while one was open for 15% of the time, Pallas kernels for 0%

profile of v1, /device:TPU:0, one launch (start us, length us, event | category | flops | bytes accessed | tf_op | source)
XLA Modules:
  0.0 418.7 jit_solution(15272837373244284159)
XLA Ops:
  7.2 0.0 all-gather.3.cloned.1.call-start
  7.2 0.7 all-gather.3.cloned.1.call-update
  7.9 0.0 all-gather.5.cloned.1.call-start
  8.0 1.5 convert_element_type.49
  9.5 0.2 convert_element_type.50
  9.7 0.1 fusion.96
  9.8 4.9 %collective-permute-start = (bf16[30,2048]{1,0:T(8,128)(2,1)S(1)}, bf16[30,2048]{1,0:T(8,128)(2,1)S(1)}, u32[]{:S(2)}, u32[]{:S(2)}) collective-permute-start(bf16[30,2048]{1,0:T(8,128)(2,1)S(1)} %fusion.96), channel_id=1, source_target_pairs={{0,8},{8,16},{16,24},{1,9},{9,17},{17,25},{2,10},{10,18},{18,26},{... | collective-permute-start | bytes 368648 | tf_op jit(solution)/shard_map/ppermute | solution.py:26
  14.7 9.1 %all_gather.9 = f32[31,2048]{1,0:T(8,128)S(1)} all-gather(f32[31,512]{1,0:T(8,128)S(1)} %copy-done.49), channel_id=1, replica_groups=mesh['sp'=4,'dp'=8] {'sp'}, dimensions={1}, use_global_device_ids=true | all-gather | bytes 317440 | tf_op jit(solution)/shard_map/all_gather | solution.py:23
  23.8 0.1 fusion.99
  24.1 0.6 fusion.87
  24.6 0.1 fusion.100
  24.8 0.3 maximum_convert_fusion
  25.3 10.7 %convert_reduce_fusion = (f32[256]{0:T(256)S(1)}, bf16[256,2048]{1,0:T(8,128)(2,1)S(1)}) fusion(f32[286,2048]{1,0:T(8,128)S(1)} %maximum_convert_fusion, f32[2048]{0:T(1024)S(1)} %bitcast.106, f32[2048]{0:T(1024)S(1)} %bitcast.108, f32[2048]{0:T(1024)S(1)} %bitcast.110, f32[2048]{0:T(1024)S(1)} %bitcast.112, f32[2048]{0:T(1024)S(1)} %bitcast.114, ...), kind=kLoop, calls=%fused_computation.37 | loop fusion | flops 33554176 | bytes 66315264 | tf_op jit(solution)/shard_map/reduce_sum | solution.py:34
  36.2 0.9 copy-done.3
  37.1 0.4 fusion.20
  37.6 56.8 %all-gather.3.cloned.1.call-done = bf16[2048,2048]{1,0:T(8,128)(2,1)} async-done(((bf16[256,2048]{1,0:T(8,128)(2,1)}), bf16[2048,2048]{1,0:T(8,128)(2,1)}) %all-gather.3.cloned.1.call-update) | async-done | bytes 8388624 | tf_op jit(solution)/shard_map/all_gather | solution.py:20
  94.4 9.5 %fusion.19 = (f32[2048]{0:T(1024)}, f32[256]{0:T(256)S(1)}, f32[256]{0:T(256)S(1)}, bf16[256,2048]{1,0:T(8,128)(2,1)}, f32[256,2048]{1,0:T(8,128)}) fusion(bf16[256,2048]{1,0:T(8,128)(2,1)} %copy-done.3, f32[256]{0:T(256)S(1)} %add_rsqrt_fusion, f32[256]{0:T(256)S(1)} %broadcast_multiply_fusion.2, f32[2048]{0:T(1024)} %param.10, ...), kind=kOutput, calls=%fused_computation.56 | convolution fusion | flops 2157966848 | bytes 13651968 | tf_op jit(solution)/shard_map/dot_general | solution.py:43
  103.9 0.0 all-gather.5.cloned.1.call-update
  103.9 2.3 copy.13
  106.2 4.4 %all-to-all-start = ((bf16[256,8,256]{0,2,1:T(8,128)(2,1)}), bf16[256,8,256]{0,2,1:T(8,128)(2,1)}, u32[]{:S(2)}, u32[]{:S(2)}) async-start(bf16[256,8,256]{0,2,1:T(8,128)(2,1)} %bitcast.102), calls=%async_computation | async-start | bytes 2097152 | tf_op jit(solution)/shard_map/all_to_all | solution.py:22
  110.6 0.0 all-reduce.3.cloned.1.call-start
  110.7 54.7 %all-to-all-done = bf16[256,8,256]{0,2,1:T(8,128)(2,1)} async-done(((bf16[256,8,256]{0,2,1:T(8,128)(2,1)}), bf16[256,8,256]{0,2,1:T(8,128)(2,1)}, u32[]{:S(2)}, u32[]{:S(2)}) %all-to-all-start) | async-done | bytes 1048608 | tf_op jit(solution)/shard_map/all_to_all | solution.py:22
  165.4 2.3 copy.14
  167.7 8.2 %fusion.55 = (f32[2048]{0:T(1024)}, f32[2048]{0:T(1024)}, f32[2048]{0:T(1024)}, f32[2048]{0:T(1024)}, f32[2048]{0:T(1024)}, /*index=5*/f32[2048]{0:T(1024)}, f32...) fusion(f32[286,2048]{1,0:T(8,128)S(1)} %maximum_convert_fusion,, ...), kind=kLoop, calls=%fused_computation.92 | loop fusion | flops 24080384 | bytes 42102784 | tf_op jit(solution)/shard_map/reduce_sum | solution.py:61
  175.9 0.7 slice.523
  176.6 1.5 collective-permute-start.1
  178.1 4.2 %fusion.54 = (f32[2048]{0:T(1024)}, f32[2048]{0:T(1024)}, f32[2048]{0:T(1024)}, f32[2048]{0:T(1024)}, f32[2048]{0:T(1024)}, /*index=5*/f32[2048]{0:T(1024)}, f32...) fusion(bf16[256,2048]{1,0:T(8,128)(2,1)S(1)} %get-tuple-element, ...), kind=kLoop, calls=%fused_computation.91 | loop fusion | flops 14129152 | bytes 28418048 | tf_op jit(solution)/shard_map/reduce_sum | solution.py:61
  182.3 6.1 %stack.131 = f32[32,2048]{1,0:T(8,128)} concatenate(f32[1,2048]{1,0:T(1,128)} %bitcast.178, f32[1,2048]{1,0:T(1,128)} %bitcast.180, f32[1,2048]{1,0:T(1,128)} %bitcast.181, f32[1,2048]{1,0:T(1,128)} %bitcast.182, f32[1,2048]{1,0:T(1,128)} %bitcast.183, f32[1,2048]{1,0:T(1,128)} %bitcast.184, f32[1,2048]{1,0:T(1,128)} %bitcast.185, f32[1,2048]{1,0:T(1,128)} %bitcast.186, ...), dimensions={0} | concatenate | bytes 524288 | tf_op jit(solution)/shard_map/stack | solution.py:62
  188.4 0.0 all-reduce.3.cloned.1.call-update
  188.5 0.0 all-reduce.5.cloned.1.call-start
  188.5 1.5 maximum_convert_fusion.1
  190.0 16.3 %all-gather.5.cloned.1.call-done = bf16[2048,2048]{1,0:T(8,128)(2,1)} async-done(((bf16[256,2048]{1,0:T(8,128)(2,1)}), bf16[2048,2048]{1,0:T(8,128)(2,1)}) %all-gather.5.cloned.1.call-update) | async-done | bytes 8388624 | tf_op jit(solution)/shard_map/all_gather | solution.py:41
  206.4 7.4 %convolution_bitcast_fusion = f32[256,2048]{0,1:T(8,128)} fusion(bf16[2048,2048]{1,0:T(8,128)(2,1)} %all-gather.5.cloned.1.call-done, bf16[2048,256]{1,0:T(8,128)(2,1)} %bitcast.103), kind=kOutput, calls=%fused_computation.31 | convolution fusion | flops 2147483648 | bytes 11534336 | tf_op jit(solution)/shard_map/dot_general | solution.py:72
  213.9 0.0 all-reduce.5.cloned.1.call-update
  213.9 0.5 copy-done.5
  214.5 0.0 copy-done.7
  214.5 0.0 copy-done.15
  214.5 0.0 copy-done.17
  214.6 0.0 copy-done.23
  214.6 0.0 copy-done.25
  214.7 0.0 copy-done.35
  214.7 10.6 %fusion.88 = (bf16[1,256,2048]{2,1,0:T(8,128)(2,1)}, bf16[256,2048]{1,0:T(8,128)(2,1)S(1)}) fusion(bf16[1,256,2048]{2,1,0:T(8,128)(2,1)} %param.6, bf16[1,256,2048]{2,1,0:T(8,128)(2,1)S(1)} %copy-done, f32[286,2048]{1,0:T(8,128)S(1)} %maximum_convert_fusion.1, f32[2048]{0:T(1024)S(1)} %bitcast.107, f32[2048]{0:T(1024)S(1)} %bitcast.109, ...), kind=kLoop, calls=%fused_computation.163 | loop fusion | flops 38273024 | bytes 69459968 | tf_op jit(solution)/shard_map/broadcast_in_dim | solution.py:76
  225.3 1.6 fusion.89
  226.8 110.4 %all-reduce.3.cloned.1.call-done = f32[32,2048]{1,0:T(8,128)} async-done(((f32[32,2048]{1,0:T(8,128)}), f32[32,2048]{1,0:T(8,128)}) %all-reduce.3.cloned.1.call-update) | async-done | bytes 262160 | tf_op jit(solution)/shard_map/psum | solution.py:62
  337.2 1.4 slice.556
  338.7 1.5 constant_dynamic-slice_fusion
  340.1 69.2 %all-reduce.5.cloned.1.call-done = f32[256,2048]{0,1:T(8,128)} async-done(((f32[256,2048]{0,1:T(8,128)}), f32[256,2048]{0,1:T(8,128)}) %all-reduce.5.cloned.1.call-update) | async-done | bytes 2097168 | tf_op jit(solution)/shard_map/psum | solution.py:75
  409.3 2.9 copy.15
  (99 shorter events, 0.3 us)
Async XLA Ops:
  7.2 2.3 copy-start
  7.2 87.2 %all-gather.3.cloned.1.call-start = ((), (), s32[]{:S(2)}) async-start(), calls=%async_computation.1 | async-start | bytes 9437184 | tf_op jit(solution)/shard_map/all_gather | solution.py:20
  7.9 198.4 %all-gather.5.cloned.1.call-start = ((), (), s32[]{:S(2)}) async-start(), calls=%async_computation.3 | async-start | bytes 9437184 | tf_op jit(solution)/shard_map/all_gather | solution.py:41
  9.4 5.3 %copy-start.49 = (f32[31,512]{1,0:T(8,128)S(1)}, f32[31,512]{1,0:T(8,128)}, u32[]{:S(2)}) copy-start(f32[31,512]{1,0:T(8,128)} %param.9) | copy-start | bytes 190468
  9.4 14.4 %copy-start.2 = (bf16[1,256,2048]{2,1,0:T(8,128)(2,1)S(1)}, bf16[1,256,2048]{2,1,0:T(8,128)(2,1)}, u32[]{:S(2)}) copy-start(bf16[1,256,2048]{2,1,0:T(8,128)(2,1)} %param.6) | copy-start | bytes 3145732
  9.8 15.0 %collective-permute-start = (bf16[30,2048]{1,0:T(8,128)(2,1)S(1)}, bf16[30,2048]{1,0:T(8,128)(2,1)S(1)}, u32[]{:S(2)}, u32[]{:S(2)}) collective-permute-start(bf16[30,2048]{1,0:T(8,128)(2,1)S(1)} %fusion.96), channel_id=1, source_target_pairs={{0,8},{8,16},{16,24},{1,9},{9,17},{17,25},{2,10},{10,18},{18,26},{... | collective-permute-start | bytes 368648 | tf_op jit(solution)/shard_map/ppermute | solution.py:26
  23.9 1.3 copy-start.4
  23.9 1.3 copy-start.6
  23.9 1.3 copy-start.8
  23.9 1.3 copy-start.10
  23.9 1.3 copy-start.12
  23.9 1.3 copy-start.14
  23.9 1.3 copy-start.16
  24.0 1.3 copy-start.18
  24.0 1.3 copy-start.20
  24.0 1.3 copy-start.22
  24.0 1.3 copy-start.24
  24.0 1.3 copy-start.26
  24.0 1.3 copy-start.28
  24.0 1.3 copy-start.30
  24.0 1.3 copy-start.32
  24.0 1.3 copy-start.34
  24.0 1.3 copy-start.36
  24.7 11.3 %copy-start.37 = (f32[1,2048]{1,0:T(1,128)}, f32[1,2048]{1,0:T(1,128)S(1)}, u32[]{:S(2)}) copy-start(f32[1,2048]{1,0:T(1,128)S(1)} %get-tuple-element.79) | copy-start | bytes 24580
  24.7 11.3 %copy-start.38 = (f32[1,2048]{1,0:T(1,128)}, f32[1,2048]{1,0:T(1,128)S(1)}, u32[]{:S(2)}) copy-start(f32[1,2048]{1,0:T(1,128)S(1)} %get-tuple-element.80) | copy-start | bytes 24580
  24.7 11.3 %copy-start.39 = (f32[1,2048]{1,0:T(1,128)}, f32[1,2048]{1,0:T(1,128)S(1)}, u32[]{:S(2)}) copy-start(f32[1,2048]{1,0:T(1,128)S(1)} %get-tuple-element.81) | copy-start | bytes 24580
  24.7 11.3 %copy-start.40 = (f32[1,2048]{1,0:T(1,128)}, f32[1,2048]{1,0:T(1,128)S(1)}, u32[]{:S(2)}) copy-start(f32[1,2048]{1,0:T(1,128)S(1)} %get-tuple-element.82) | copy-start | bytes 24580
  24.7 11.3 %copy-start.41 = (f32[1,2048]{1,0:T(1,128)}, f32[1,2048]{1,0:T(1,128)S(1)}, u32[]{:S(2)}) copy-start(f32[1,2048]{1,0:T(1,128)S(1)} %get-tuple-element.83) | copy-start | bytes 24580
  24.8 11.3 %copy-start.42 = (f32[1,2048]{1,0:T(1,128)}, f32[1,2048]{1,0:T(1,128)S(1)}, u32[]{:S(2)}) copy-start(f32[1,2048]{1,0:T(1,128)S(1)} %get-tuple-element.84) | copy-start | bytes 24580
  24.8 11.3 %copy-start.43 = (f32[1,2048]{1,0:T(1,128)}, f32[1,2048]{1,0:T(1,128)S(1)}, u32[]{:S(2)}) copy-start(f32[1,2048]{1,0:T(1,128)S(1)} %get-tuple-element.85) | copy-start | bytes 24580
  24.8 11.3 %copy-start.44 = (f32[1,2048]{1,0:T(1,128)}, f32[1,2048]{1,0:T(1,128)S(1)}, u32[]{:S(2)}) copy-start(f32[1,2048]{1,0:T(1,128)S(1)} %get-tuple-element.86) | copy-start | bytes 24580
  24.8 11.3 %copy-start.45 = (f32[1,2048]{1,0:T(1,128)}, f32[1,2048]{1,0:T(1,128)S(1)}, u32[]{:S(2)}) copy-start(f32[1,2048]{1,0:T(1,128)S(1)} %get-tuple-element.87) | copy-start | bytes 24580
  24.8 11.3 %copy-start.46 = (f32[1,2048]{1,0:T(1,128)}, f32[1,2048]{1,0:T(1,128)S(1)}, u32[]{:S(2)}) copy-start(f32[1,2048]{1,0:T(1,128)S(1)} %get-tuple-element.88) | copy-start | bytes 24580
  24.8 11.3 %copy-start.47 = (f32[1,2048]{1,0:T(1,128)}, f32[1,2048]{1,0:T(1,128)S(1)}, u32[]{:S(2)}) copy-start(f32[1,2048]{1,0:T(1,128)S(1)} %get-tuple-element.89) | copy-start | bytes 24580
  24.8 11.3 %copy-start.48 = (f32[1,2048]{1,0:T(1,128)}, f32[1,2048]{1,0:T(1,128)S(1)}, u32[]{:S(2)}) copy-start(f32[1,2048]{1,0:T(1,128)S(1)} %get-tuple-element.90) | copy-start | bytes 24580
  36.2 1.0 copy-start.3
  106.2 61.5 %copy-start.50 = (f32[2048]{0:T(1024)S(1)}, f32[2048]{0:T(1024)}, u32[]{:S(2)}) copy-start(f32[2048]{0:T(1024)} %param.10) | copy-start | bytes 24580
  106.2 59.1 %all-to-all-start = ((bf16[256,8,256]{0,2,1:T(8,128)(2,1)}), bf16[256,8,256]{0,2,1:T(8,128)(2,1)}, u32[]{:S(2)}, u32[]{:S(2)}) async-start(bf16[256,8,256]{0,2,1:T(8,128)(2,1)} %bitcast.102), calls=%async_computation | async-start | bytes 2097152 | tf_op jit(solution)/shard_map/all_to_all | solution.py:22
  110.6 226.6 %all-reduce.3.cloned.1.call-start = ((), (), s32[]{:S(2)}) async-start(), calls=%async_computation.2 | async-start | bytes 524288 | tf_op jit(solution)/shard_map/psum | solution.py:62
  175.9 6.4 %copy-start.1 = (bf16[256,2048]{1,0:T(8,128)(2,1)}, bf16[256,2048]{1,0:T(8,128)(2,1)S(1)}, u32[]{:S(2)}) copy-start(bf16[256,2048]{1,0:T(8,128)(2,1)S(1)} %get-tuple-element.54) | copy-start | bytes 3145732
  176.6 11.9 %collective-permute-start.1 = (bf16[30,2048]{1,0:T(8,128)(2,1)}, bf16[30,2048]{1,0:T(8,128)(2,1)S(1)}, u32[]{:S(2)}, u32[]{:S(2)}) collective-permute-start(bf16[30,2048]{1,0:T(8,128)(2,1)} %slice.523), channel_id=1, source_target_pairs={{8,0},{16,8},{24,16},{9,1},{17,9},{25,17},{10,2},{18,10},{26,18},{... | collective-permute-start | bytes 368648 | tf_op jit(solution)/shard_map/ppermute | solution.py:53
  188.5 220.8 %all-reduce.5.cloned.1.call-start = ((), (), s32[]{:S(2)}) async-start(), calls=%async_computation.4 | async-start | bytes 4194304 | tf_op jit(solution)/shard_map/psum | solution.py:75
  213.8 0.8 copy-start.25
  213.8 0.8 copy-start.27
  213.9 0.8 copy-start.29
  213.9 0.8 copy-start.31
  213.9 0.8 copy-start.33
  213.9 0.8 copy-start.35
  (10 other events, 7.5 us)
Sparse Core Ops, SparseCore 0:
  9.6 84.7 all-gather.2
  104.0 102.3 all-gather.4
  211.9 125.3 all-reduce.2
  340.8 68.5 all-reduce.4

commit v2 on v1

v2 whole, which is shorter than its diff:
```python
import functools

import jax
import jax.numpy as jnp
from jax import lax
from jax.experimental import pallas as pl
from jax.experimental.pallas import tpu as pltpu
from jax.sharding import PartitionSpec as P

NORM_EPS = 1e-05
VMEM = pl.BlockSpec(memory_space=pltpu.VMEM)


class Copies:
    def __init__(self, send, recv, local):
        self.send, self.recv, self.local = send, recv, local
        self.n_remote = self.n_local = 0
        self.remote, self.locals = [], []

    def start(self, src, dst, target):
        i = self.n_remote
        self.n_remote += 1
        copy = pltpu.make_async_remote_copy(
            src_ref=src,
            dst_ref=dst,
            send_sem=self.send.at[i],
            recv_sem=self.recv.at[i],
            device_id=target,
            device_id_type=pl.DeviceIdType.MESH,
        )
        copy.start()
        self.remote.append([copy, False])
        return len(self.remote) - 1

    def keep(self, src, dst):
        copy = pltpu.make_async_copy(src, dst, self.local.at[self.n_local])
        self.n_local += 1
        copy.start()
        self.locals.append(copy)

    def arrive(self, i):
        self.remote[i][0].wait_recv()
        self.remote[i][1] = True

    def finish(self):
        for copy, arrived in self.remote:
            if not arrived:
                copy.wait_recv()
            copy.wait_send()
        for copy in self.locals:
            copy.wait()


def greet(axes):
    barrier = pltpu.get_barrier_semaphore()
    count = 0
    for axis in axes:
        n = lax.axis_size(axis)
        me = lax.axis_index(axis)
        for k in range(1, n):
            pl.semaphore_signal(
                barrier,
                inc=1,
                device_id={axis: lax.rem(me + k, n)},
                device_id_type=pl.DeviceIdType.MESH,
            )
            count += 1
    pl.semaphore_wait(barrier, count)


def direct(copies, kind, axis, src, dst):
    n = lax.axis_size(axis)
    me = lax.axis_index(axis)
    if kind == "next" or kind == "prev":
        copies.start(src, dst, {axis: lax.rem(me + (1 if kind == "next" else n - 1), n)})
        return
    copies.keep(src.at[me] if kind == "scatter" else src, dst.at[me])
    for k in range(1, n):
        peer = lax.rem(me + k, n)
        copies.start(src.at[peer] if kind == "scatter" else src, dst.at[me], {axis: peer})


def spread_gather(copies, src, dst):
    ns, nz = lax.axis_size("sp"), lax.axis_size("dp") // 2
    s, d = lax.axis_index("sp"), lax.axis_index("dp")
    z, c = d // 2, lax.rem(d, 2)
    partner = {"dp": d + 1 - 2 * c}
    first = [
        copies.start(src.at[s], dst.at[d, s], {"dp": 2 * lax.rem(z + k, nz) + c})
        for k in range(1, nz)
    ]
    copies.keep(src, dst.at[d])
    copies.start(src, dst.at[d], partner)
    second = {}
    for k in range(1, nz):
        copies.arrive(first[k - 1])
        piece = dst.at[2 * lax.rem(z + nz - k, nz) + c, s]
        for j in range(1, ns):
            second[k, j] = copies.start(piece, piece, {"sp": lax.rem(s + j, ns)})
        copies.start(piece, piece, partner)
    for k in range(1, nz):
        for j in range(1, ns):
            copies.arrive(second[k, j])
            piece = dst.at[2 * lax.rem(z + nz - k, nz) + c, lax.rem(s + ns - j, ns)]
            copies.start(piece, piece, partner)


def ring_gather(copies, src, dst):
    nz = lax.axis_size("dp") // 2
    d = lax.axis_index("dp")
    z, c = d // 2, lax.rem(d, 2)
    partner = {"dp": d + 1 - 2 * c}
    up = {"dp": 2 * lax.rem(z + 1, nz) + c}
    down = {"dp": 2 * lax.rem(z + nz - 1, nz) + c}
    a = copies.start(src.at[0], dst.at[d, 0], up)
    b = copies.start(src.at[1], dst.at[d, 1], down)
    copies.keep(src, dst.at[d])
    copies.start(src, dst.at[d], partner)
    for k in range(1, nz):
        low = dst.at[2 * lax.rem(z + nz - k, nz) + c, 0]
        high = dst.at[2 * lax.rem(z + k, nz) + c, 1]
        copies.arrive(a)
        if k < nz - 1:
            a = copies.start(low, low, up)
        copies.arrive(b)
        if k < nz - 1:
            b = copies.start(high, high, down)
        copies.start(low, low, partner)
        copies.start(high, high, partner)


def run(axes, items, *refs):
    n = len(items)
    copies = Copies(*refs[2 * n :])
    greet(axes)
    for i, (kind, axis) in enumerate(items):
        src, dst = refs[i], refs[n + i]
        if kind == "spread":
            spread_gather(copies, src, dst)
        elif kind == "ring":
            ring_gather(copies, src, dst)
        else:
            direct(copies, kind, axis, src, dst)
    copies.finish()


def exchange(collective_id, *items):
    ns, nd = lax.axis_size("sp"), lax.axis_size("dp")
    shapes, remote, local = [], 0, 0
    for kind, axis, x in items:
        n = lax.axis_size(axis)
        if kind in ("next", "prev"):
            shape = x.shape
            remote += 1
        elif kind == "scatter":
            shape = x.shape
            remote += n - 1
            local += 1
        else:
            shape = (n,) + x.shape
            local += 1
            if kind == "gather":
                remote += n - 1
            elif kind == "spread":
                remote += (nd // 2 - 1) * 2 * ns + 1
            else:
                remote += (nd // 2 - 1) * 4 + 1
        shapes.append(jax.ShapeDtypeStruct(shape, x.dtype))
    axes = tuple(a for a in ("sp", "dp") if any(axis == a or kind == "spread" for kind, axis, _ in items))
    return pl.pallas_call(
        functools.partial(run, axes, tuple((kind, axis) for kind, axis, _ in items)),
        out_shape=shapes,
        in_specs=[VMEM] * len(items),
        out_specs=[VMEM] * len(items),
        scratch_shapes=[
            pltpu.SemaphoreType.DMA((remote,)),
            pltpu.SemaphoreType.DMA((remote,)),
            pltpu.SemaphoreType.DMA((max(local, 1),)),
        ],
        compiler_params=pltpu.CompilerParams(
            collective_id=collective_id, has_side_effects=True, vmem_limit_bytes=48 * 1024 * 1024
        ),
    )(*[x for _, _, x in items])


def body(value_half, gate_half, upstream, conv_taps, norm_gain, out_weight):
    f32 = jnp.float32
    tap_count = conv_taps.shape[0]
    halo = tap_count - 1
    nsp, ndp = lax.axis_size("sp"), lax.axis_size("dp")
    at_start = lax.axis_index("sp") == 0
    at_end = lax.axis_index("sp") == nsp - 1
    edge = (halo + 15) // 16 * 16

    value = value_half[0].astype(f32)
    gate = gate_half[0].astype(f32)
    length = value.shape[0]
    channels = value.shape[1]
    up = upstream[0]
    rows = out_weight.shape[0]

    tail = (value[length - edge :] * jax.nn.sigmoid(gate[length - edge :])).astype(jnp.bfloat16)
    up_blocks = jnp.swapaxes(up.reshape(length, ndp, rows), 0, 1)
    before, taps, up_columns, weight = exchange(
        1,
        ("next", "sp", tail),
        ("gather", "sp", conv_taps),
        ("scatter", "dp", up_blocks),
        ("spread", "dp", out_weight.reshape(nsp, rows // nsp, channels)),
    )
    before = jnp.where(at_start, 0, before)[edge - halo :]
    taps = jnp.swapaxes(taps, 0, 1).reshape(tap_count, channels)
    up_columns = up_columns.reshape(ndp * length, rows)
    weight = weight.reshape(ndp * rows, channels)
    sig_gate = jax.nn.sigmoid(gate)
    glu = (value * sig_gate).astype(jnp.bfloat16)
    padded = jnp.concatenate([before, glu], axis=0).astype(f32)
    conv = jnp.zeros((length, padded.shape[1]), f32)
    for j in range(tap_count):
        conv = conv + taps[j] * padded[j : j + length]
    conv = conv.astype(jnp.bfloat16).astype(f32)
    mean = jnp.mean(conv, axis=-1, keepdims=True)
    centered = conv - mean
    inv = lax.rsqrt(jnp.mean(centered * centered, axis=-1, keepdims=True) + NORM_EPS)
    normed = centered * inv
    scaled = normed * norm_gain
    sig = jax.nn.sigmoid(scaled)
    activated = (scaled * sig).astype(jnp.bfloat16)

    grad_act = jnp.dot(up, weight, preferred_element_type=f32)
    grad_scaled = grad_act * sig * (1.0 + scaled * (1.0 - sig))
    gain_part = jnp.sum(grad_scaled * normed, axis=0)
    g = grad_scaled * norm_gain
    grad_conv = inv * (
        g
        - jnp.mean(g, axis=-1, keepdims=True)
        - normed * jnp.mean(g * normed, axis=-1, keepdims=True)
    )
    grad_conv = grad_conv.astype(jnp.bfloat16)
    after, act_all = exchange(
        2,
        ("prev", "sp", grad_conv[:edge]),
        ("ring", "dp", activated.reshape(2, length // 2, channels)),
    )
    after = jnp.where(at_end, 0, after)[:halo]
    act_all = act_all.reshape(ndp * length, channels)
    extended = jnp.concatenate([grad_conv, after], axis=0).astype(f32)
    here = grad_conv.astype(f32)
    grad_glu = jnp.zeros_like(here)
    terms = []
    for j in range(tap_count):
        first = halo - j
        grad_glu = grad_glu + taps[j] * extended[first : first + length]
        terms.append(jnp.sum(here * padded[j : j + length], axis=0))
    grad_glu = grad_glu.astype(jnp.bfloat16).astype(f32)
    grad_value = (grad_glu * sig_gate).astype(jnp.bfloat16)
    grad_gate = (grad_glu * value * sig_gate * (1.0 - sig_gate)).astype(jnp.bfloat16)

    owned = lax.dot_general(
        up_columns, act_all, (((0,), (0,)), ((), ())), preferred_element_type=f32
    )
    width = conv_taps.shape[1]
    tap_blocks = jnp.swapaxes(jnp.stack(terms).reshape(tap_count, nsp, width), 0, 1)
    gain_got, tap_got, owned_got = exchange(
        3,
        ("gather", "sp", gain_part[None]),
        ("scatter", "sp", tap_blocks),
        ("scatter", "sp", owned.astype(jnp.bfloat16).reshape(nsp, rows // nsp, channels)),
    )
    gain_got, tap_got, grad_weight = exchange(
        4,
        ("gather", "dp", jnp.sum(gain_got, axis=0)),
        ("gather", "dp", jnp.sum(tap_got, axis=0)),
        ("gather", "sp", jnp.sum(owned_got.astype(f32), axis=0).astype(jnp.bfloat16)),
    )
    grad_gain = jnp.sum(gain_got, axis=0)[0]
    grad_taps = jnp.sum(tap_got, axis=0)
    grad_weight = grad_weight.reshape(rows, channels).astype(f32)
    return (grad_value[None], grad_gate[None], grad_taps, grad_gain, grad_weight)


def solution(mesh):
    tokens = P("dp", "sp", None)
    return jax.shard_map(
        body,
        mesh=mesh,
        in_specs=(tokens, tokens, tokens, P(None, "sp"), P(), P("dp", None)),
        out_specs=(tokens, tokens, P(None, "sp"), P(), P("dp", None)),
        check_vma=False,
    )
```

time: 419 us -> 261 us (0.62)
  waiting for transfers between devices: 308 us -> 0 us
  Pallas kernels: 0 us -> 199 us
  between operations: 14.5 us -> 1.34 us
  starting transfers between devices: 10.9 us -> 0 us
  local copies, waits for them, and re-layouts: 19.3 us -> 9.86 us
  blocking collectives: 9.08 us -> 0 us
  matrix products: 16.9 us -> 11.6 us
    pallas_call x0 -> x4, Pallas kernels: none -> 199 us  [exchange(): pl.pallas_call(functools.partial(run, axes, tuple(((kind, axis) for kind,...]
    psum x2 -> x0, waiting for transfers between devices: 180 us -> none  [the longest x1 110 us: body(): sums = lax.psum(jnp.stack(terms + [gain_part]), ('sp', 'dp'))]
    all_gather x2 -> x0, waiting for transfers between devices: 73.1 us -> none  [the longest x1 56.8 us: body(): weight = lax.all_gather(out_weight, 'dp', axis=0, tiled=True)]
    all_to_all x1 -> x0, waiting for transfers between devices: 54.7 us -> none  [body(): lax.all_to_all(up, 'dp', split_axis=1, concat_axis=0, tiled=True)]
    all_gather x1 -> x0, blocking collectives: 9.08 us -> none  [body(): taps = lax.all_gather(conv_taps, 'sp', axis=1, tiled=True)]
    ppermute x2 -> x0, starting transfers between devices: 6.34 us -> none  [the longest x1 4.88 us: body(): before = lax.ppermute(tail, 'sp', onward)]
    all_to_all x1 -> x0, starting transfers between devices: 4.39 us -> none  [body(): lax.all_to_all(up, 'dp', split_axis=1, concat_axis=0, tiled=True)]
  transfers between devices with their start and end apart: 7 -> 0, of which waited for: 5 -> 0; matrix products, arithmetic and copies ran while one was open for 15% -> 0% of each run, Pallas kernels for 0% -> 0%
where the time goes in v2:
time: 261 us
  Pallas kernels  199 us (76%)
  other arithmetic  38.8 us (15%)
  matrix products  11.6 us (4%)
  local copies, waits for them, and re-layouts  9.86 us (4%)
    pallas_call x4, Pallas kernels, exchange(): pl.pallas_call(functools.partial(run, axes, tuple(((kind, axis) for kind,...  199 us
    reduce_sum x2, other arithmetic, body(): terms.append(jnp.sum(here * padded[j:j + length], axis=0))  11.4 us
    reduce_sum x1, other arithmetic, body(): mean = jnp.mean(conv, axis=-1, keepdims=True)  10.9 us
    broadcast_in_dim x1, other arithmetic, body(): grad_gate[None]  9.47 us
    dot_general x1, matrix products, body(): grad_act = jnp.dot(up, weight, preferred_element_type=f32)  5.89 us
    dot_general x1, matrix products, body(): lax.dot_general(up_columns, act_all, (((0,), (0,)), ((), ())), preferred_...  5.73 us

profile of v2, /device:TPU:0, one launch (start us, length us, event | category | flops | bytes accessed | tf_op | source)
XLA Modules:
  0.0 260.8 jit_solution(338509100323837696)
XLA Ops:
  0.6 0.0 copy-start.2
  0.7 0.0 copy-start.4
  0.7 2.4 copy.11
  3.1 1.5 copy.12
  4.6 0.6 fusion.88
  5.1 0.2 convert_element_type.63
  5.4 0.0 copy-start
  5.4 0.0 copy-start.1
  5.4 0.2 convert_element_type.64
  5.6 0.1 fusion.97.refs_0_
  5.7 0.9 copy-done
  6.6 76.2 %shard_map.101 = (bf16[32,2048]{1,0:T(8,128)(2,1)S(1)}, f32[4,31,512]{2,1,0:T(8,128)S(1)}, bf16[8,256,256]{2,1,0:T(8,128)(2,1)S(1)}, bf16[8,4,64,2048]{3,2,1,0:T(8,128)(2,1)}) custom-call(bf16[32,2048]{1,0:T(8,128)(2,1)S(1)} %fusion.97.refs_0_, f32[31,512]{1,0:T(8,128)S(1)} %copy-done.1, bf16[8,256,256]{2,1,0:T(8,128)(2,1)S(1)} %bitcast.116, ...), custom_call_target="tpu_custom_call" | custom-call | tf_op jit(solution)/shard_map/pallas_call | solution.py:170
  82.8 0.1 fusion.101
  82.9 0.1 fusion.100
  83.2 0.3 maximum_convert_fusion
  83.5 0.0 copy-start.6
  83.6 0.0 copy-start.35
  83.6 10.9 %convert_reduce_fusion = (f32[256]{0:T(256)S(1)}, bf16[256,2048]{1,0:T(8,128)(2,1)S(1)}) fusion(f32[286,2048]{1,0:T(8,128)S(1)} %maximum_convert_fusion, f32[2048]{0:T(1024)S(1)} %bitcast.153, f32[2048]{0:T(1024)S(1)} %bitcast.155, f32[2048]{0:T(1024)S(1)} %bitcast.157, f32[2048]{0:T(1024)S(1)} %bitcast.159, f32[2048]{0:T(1024)S(1)} %bitcast.161, ...), kind=kLoop, calls=%fused_computation.37 | loop fusion | flops 33554176 | bytes 66315264 | tf_op jit(solution)/shard_map/reduce_sum | solution.py:222
  94.5 0.0 copy-done.7
  94.5 0.0 copy-done.9
  94.5 0.0 copy-done.11
  94.5 0.0 copy-done.13
  94.5 0.0 copy-done.15
  94.6 0.0 copy-done.17
  94.6 0.0 copy-done.19
  94.6 0.0 copy-done.21
  94.6 0.0 copy-done.23
  94.6 0.0 copy-done.25
  94.7 0.4 fusion.21
  95.1 5.9 %fusion.20 = (f32[2048]{0:T(1024)S(1)}, f32[256]{0:T(256)S(1)}, f32[256]{0:T(256)S(1)}, bf16[256,2048]{1,0:T(8,128)(2,1)S(1)}, f32[256,2048]{1,0:T(8,128)S(1)}) fusion(bf16[256,2048]{1,0:T(8,128)(2,1)S(1)} %get-tuple-element.67, f32[256]{0:T(256)S(1)} %add_rsqrt_fusion, f32[256]{0:T(256)S(1)} %broadcast_multiply_fusion.2, f32[2048]{0:T(1024)S(1)} %copy-done.35, ...), kind=kOutput, calls=%fused_computation.57 | convolution fusion | flops 2157966848 | bytes 13651968 | tf_op jit(solution)/shard_map/dot_general | solution.py:230
  101.0 7.2 %fusion.56 = (f32[2048]{0:T(1024)}, f32[2048]{0:T(1024)}, f32[2048]{0:T(1024)}, f32[2048]{0:T(1024)}, f32[2048]{0:T(1024)}, /*index=5*/f32[2048]{0:T(1024)}, f32...) fusion(f32[286,2048]{1,0:T(8,128)S(1)} %maximum_convert_fusion,, ...), kind=kLoop, calls=%fused_computation.93 | loop fusion | flops 24080384 | bytes 42102784 | tf_op jit(solution)/shard_map/reduce_sum | solution.py:254
  108.2 4.2 %fusion.55 = (f32[2048]{0:T(1024)}, f32[2048]{0:T(1024)}, f32[2048]{0:T(1024)}, f32[2048]{0:T(1024)}, f32[2048]{0:T(1024)}, /*index=5*/f32[2048]{0:T(1024)}, f32...) fusion(bf16[256,2048]{1,0:T(8,128)(2,1)S(1)} %get-tuple-element, ...), kind=kLoop, calls=%fused_computation.92 | loop fusion | flops 14129152 | bytes 28418048 | tf_op jit(solution)/shard_map/reduce_sum | solution.py:254
  112.4 3.6 %stack.127 = f32[31,4,512]{2,0,1:T(8,128)S(1)} concatenate(f32[1,4,512]{2,0,1:T(1,128)} %bitcast.201, f32[1,4,512]{2,0,1:T(1,128)} %bitcast.203, f32[1,4,512]{2,0,1:T(1,128)} %bitcast.204, f32[1,4,512]{2,0,1:T(1,128)} %bitcast.205, f32[1,4,512]{2,0,1:T(1,128)} %bitcast.206, f32[1,4,512]{2,0,1:T(1,128)} %bitcast.207, f32[1,4,512]{2,0,1:T(1,128)} %bitcast.208, ...), dimensions={0} | concatenate | bytes 507904 | tf_op jit(solution)/shard_map/stack | solution.py:263
  116.1 88.3 %shard_map.102 = (bf16[32,2048]{1,0:T(8,128)(2,1)S(1)}, bf16[8,2,128,2048]{3,2,1,0:T(8,128)(2,1)}) custom-call(bf16[32,2048]{1,0:T(8,128)(2,1)S(1)} %slice.555.refs_0_, bf16[2,128,2048]{2,1,0:T(8,128)(2,1)S(1)} %bitcast.119), custom_call_target="tpu_custom_call" | custom-call | tf_op jit(solution)/shard_map/pallas_call | solution.py:170
  204.4 5.7 %convolution_convert_fusion = bf16[256,2048]{1,0:T(8,128)(2,1)S(1)} fusion(bf16[2048,256]{1,0:T(8,128)(2,1)S(1)} %bitcast.117, bf16[2048,2048]{1,0:T(8,128)(2,1)} %bitcast.125), kind=kOutput, calls=%fused_computation.38 | convolution fusion | flops 2148007936 | bytes 10485760 | tf_op jit(solution)/shard_map/dot_general | solution.py:259
  210.2 18.3 %shard_map.103 = (f32[4,1,2048]{2,1,0:T(1,128)S(1)}, f32[4,31,512]{2,1,0:T(8,128)S(1)}, bf16[4,64,2048]{2,1,0:T(8,128)(2,1)S(1)}) custom-call(f32[1,2048]{1,0:T(1,128)S(1)} %bitcast.124, f32[4,31,512]{2,1,0:T(8,128)S(1)} %bitcast.118, bf16[4,64,2048]{2,1,0:T(8,128)(2,1)S(1)} %bitcast.115), custom_call_target="tpu_custom_call" | custom-call | tf_op jit(solution)/shard_map/pallas_call | solution.py:170
  228.6 0.2 reduce_sum.413.refs_2_
  228.8 0.0 copy-start.3
  228.8 0.0 copy-start.5
  228.9 0.3 maximum_convert_fusion.1
  229.2 0.8 copy-done.3
  230.0 0.3 copy-done.5
  230.4 9.5 %fusion.89 = (bf16[1,256,2048]{2,1,0:T(8,128)(2,1)}, bf16[256,2048]{1,0:T(8,128)(2,1)S(1)}) fusion(bf16[1,256,2048]{2,1,0:T(8,128)(2,1)S(1)} %copy-done.5, bf16[1,256,2048]{2,1,0:T(8,128)(2,1)S(1)} %copy-done.3, f32[286,2048]{1,0:T(8,128)S(1)} %maximum_convert_fusion.1, f32[2048]{0:T(1024)S(1)} %bitcast.154, f32[2048]{0:T(1024)S(1)} %bitcast.156, ...), kind=kLoop, calls=%fused_computation.164 | loop fusion | flops 38273024 | bytes 69459968 | tf_op jit(solution)/shard_map/broadcast_in_dim | solution.py:279
  239.9 1.6 fusion.90
  241.5 16.4 %shard_map.104 = (f32[8,1,2048]{2,1,0:T(1,128)S(1)}, f32[8,31,512]{2,1,0:T(8,128)S(1)}, bf16[4,64,2048]{2,1,0:T(8,128)(2,1)S(1)}) custom-call(f32[1,2048]{1,0:T(1,128)S(1)} %bitcast.123, f32[31,512]{1,0:T(8,128)S(1)} %reduce_sum.412.refs_1_, bf16[64,2048]{1,0:T(8,128)(2,1)S(1)} %reduce_sum.413.refs_2_), custom_call_target="tpu_custom_call" | custom-call | tf_op jit(solution)/shard_map/pallas_call | solution.py:170
  257.9 0.7 reduce_sum.414
  258.6 0.7 reduce_sum.415
  259.2 1.6 bitcast_convert_fusion
  (59 shorter events, 0.3 us)
Async XLA Ops:
  0.6 3.9 %copy-start.2 = (bf16[1,256,2048]{2,1,0:T(8,128)(2,1)S(1)}, bf16[1,256,2048]{2,1,0:T(8,128)(2,1)}, u32[]{:S(2)}) copy-start(bf16[1,256,2048]{2,1,0:T(8,128)(2,1)} %param.7) | copy-start | bytes 3145732
  0.7 3.9 %copy-start.4 = (bf16[1,256,2048]{2,1,0:T(8,128)(2,1)S(1)}, bf16[1,256,2048]{2,1,0:T(8,128)(2,1)}, u32[]{:S(2)}) copy-start(bf16[1,256,2048]{2,1,0:T(8,128)(2,1)} %param.6) | copy-start | bytes 3145732
  5.4 1.2 copy-start
  5.4 1.2 copy-start.1
  83.0 11.5 %copy-start.7 = (f32[1,4,512]{2,0,1:T(1,128)}, f32[1,4,512]{2,0,1:T(1,128)S(1)}, u32[]{:S(2)}) copy-start(f32[1,4,512]{2,0,1:T(1,128)S(1)} %get-tuple-element.74) | copy-start | bytes 24580
  83.0 11.5 %copy-start.9 = (f32[1,4,512]{2,0,1:T(1,128)}, f32[1,4,512]{2,0,1:T(1,128)S(1)}, u32[]{:S(2)}) copy-start(f32[1,4,512]{2,0,1:T(1,128)S(1)} %get-tuple-element.75) | copy-start | bytes 24580
  83.1 11.5 %copy-start.11 = (f32[1,4,512]{2,0,1:T(1,128)}, f32[1,4,512]{2,0,1:T(1,128)S(1)}, u32[]{:S(2)}) copy-start(f32[1,4,512]{2,0,1:T(1,128)S(1)} %get-tuple-element.76) | copy-start | bytes 24580
  83.1 11.5 %copy-start.13 = (f32[1,4,512]{2,0,1:T(1,128)}, f32[1,4,512]{2,0,1:T(1,128)S(1)}, u32[]{:S(2)}) copy-start(f32[1,4,512]{2,0,1:T(1,128)S(1)} %get-tuple-element.77) | copy-start | bytes 24580
  83.1 11.5 %copy-start.15 = (f32[1,4,512]{2,0,1:T(1,128)}, f32[1,4,512]{2,0,1:T(1,128)S(1)}, u32[]{:S(2)}) copy-start(f32[1,4,512]{2,0,1:T(1,128)S(1)} %get-tuple-element.78) | copy-start | bytes 24580
  83.1 11.5 %copy-start.17 = (f32[1,4,512]{2,0,1:T(1,128)}, f32[1,4,512]{2,0,1:T(1,128)S(1)}, u32[]{:S(2)}) copy-start(f32[1,4,512]{2,0,1:T(1,128)S(1)} %get-tuple-element.79) | copy-start | bytes 24580
  83.1 11.5 %copy-start.19 = (f32[1,4,512]{2,0,1:T(1,128)}, f32[1,4,512]{2,0,1:T(1,128)S(1)}, u32[]{:S(2)}) copy-start(f32[1,4,512]{2,0,1:T(1,128)S(1)} %get-tuple-element.80) | copy-start | bytes 24580
  83.1 11.5 %copy-start.21 = (f32[1,4,512]{2,0,1:T(1,128)}, f32[1,4,512]{2,0,1:T(1,128)S(1)}, u32[]{:S(2)}) copy-start(f32[1,4,512]{2,0,1:T(1,128)S(1)} %get-tuple-element.81) | copy-start | bytes 24580
  83.1 11.5 %copy-start.23 = (f32[1,4,512]{2,0,1:T(1,128)}, f32[1,4,512]{2,0,1:T(1,128)S(1)}, u32[]{:S(2)}) copy-start(f32[1,4,512]{2,0,1:T(1,128)S(1)} %get-tuple-element.82) | copy-start | bytes 24580
  83.1 11.5 %copy-start.25 = (f32[1,4,512]{2,0,1:T(1,128)}, f32[1,4,512]{2,0,1:T(1,128)S(1)}, u32[]{:S(2)}) copy-start(f32[1,4,512]{2,0,1:T(1,128)S(1)} %get-tuple-element.83) | copy-start | bytes 24580
  83.1 11.5 %copy-start.27 = (f32[1,4,512]{2,0,1:T(1,128)}, f32[1,4,512]{2,0,1:T(1,128)S(1)}, u32[]{:S(2)}) copy-start(f32[1,4,512]{2,0,1:T(1,128)S(1)} %get-tuple-element.84) | copy-start | bytes 24580
  83.1 11.5 %copy-start.29 = (f32[1,4,512]{2,0,1:T(1,128)}, f32[1,4,512]{2,0,1:T(1,128)S(1)}, u32[]{:S(2)}) copy-start(f32[1,4,512]{2,0,1:T(1,128)S(1)} %get-tuple-element.85) | copy-start | bytes 24580
  83.2 11.5 %copy-start.31 = (f32[1,4,512]{2,0,1:T(1,128)}, f32[1,4,512]{2,0,1:T(1,128)S(1)}, u32[]{:S(2)}) copy-start(f32[1,4,512]{2,0,1:T(1,128)S(1)} %get-tuple-element.86) | copy-start | bytes 24580
  83.2 11.5 %copy-start.33 = (f32[1,4,512]{2,0,1:T(1,128)}, f32[1,4,512]{2,0,1:T(1,128)S(1)}, u32[]{:S(2)}) copy-start(f32[1,4,512]{2,0,1:T(1,128)S(1)} %get-tuple-element.87) | copy-start | bytes 24580
  83.5 11.5 %copy-start.6 = (bf16[1,256,2048]{2,1,0:T(8,128)(2,1)S(1)}, bf16[1,256,2048]{2,1,0:T(8,128)(2,1)}, u32[]{:S(2)}) copy-start(bf16[1,256,2048]{2,1,0:T(8,128)(2,1)} %param.8) | copy-start | bytes 3145732
  83.6 11.5 %copy-start.35 = (f32[2048]{0:T(1024)S(1)}, f32[2048]{0:T(1024)}, u32[]{:S(2)}) copy-start(f32[2048]{0:T(1024)} %param.10) | copy-start | bytes 24580
  228.8 1.2 copy-start.3
  228.8 1.5 copy-start.5
  228.8 1.5 copy-start.8
  228.8 1.5 copy-start.10
  228.8 1.5 copy-start.12
  228.8 1.5 copy-start.14
  228.8 1.5 copy-start.16
  228.8 1.5 copy-start.18
  228.9 1.5 copy-start.20
  228.9 1.5 copy-start.22
  228.9 1.5 copy-start.24
  228.9 1.5 copy-start.26
  228.9 1.5 copy-start.28
  228.9 1.5 copy-start.30
  228.9 1.5 copy-start.32
  228.9 1.5 copy-start.34

commit v3 on v2

--- a/solution.py
+++ b/solution.py
@@ -11,13 +11,20 @@
 VMEM = pl.BlockSpec(memory_space=pltpu.VMEM)
 
 
+def when(condition, act):
+    if condition is None:
+        act()
+    else:
+        pl.when(condition)(lambda: act())
+
+
 class Copies:
     def __init__(self, send, recv, local):
         self.send, self.recv, self.local = send, recv, local
         self.n_remote = self.n_local = 0
         self.remote, self.locals = [], []
 
-    def start(self, src, dst, target):
+    def start(self, src, dst, target, sends=None, receives=None):
         i = self.n_remote
         self.n_remote += 1
         copy = pltpu.make_async_remote_copy(
@@ -28,8 +35,8 @@
             device_id=target,
             device_id_type=pl.DeviceIdType.MESH,
         )
-        copy.start()
-        self.remote.append([copy, False])
+        when(sends, copy.start)
+        self.remote.append([copy, False, sends, receives])
         return len(self.remote) - 1
 
     def keep(self, src, dst):
@@ -39,14 +46,14 @@
         self.locals.append(copy)
 
     def arrive(self, i):
-        self.remote[i][0].wait_recv()
+        when(self.remote[i][3], self.remote[i][0].wait_recv)
         self.remote[i][1] = True
 
     def finish(self):
-        for copy, arrived in self.remote:
+        for copy, arrived, sends, receives in self.remote:
             if not arrived:
-                copy.wait_recv()
-            copy.wait_send()
+                when(receives, copy.wait_recv)
+            when(sends, copy.wait_send)
         for copy in self.locals:
             copy.wait()
 
@@ -89,6 +96,7 @@
         copies.start(src.at[s], dst.at[d, s], {"dp": 2 * lax.rem(z + k, nz) + c})
         for k in range(1, nz)
     ]
+    yield
     copies.keep(src, dst.at[d])
     copies.start(src, dst.at[d], partner)
     second = {}
@@ -98,6 +106,7 @@
         for j in range(1, ns):
             second[k, j] = copies.start(piece, piece, {"sp": lax.rem(s + j, ns)})
         copies.start(piece, piece, partner)
+    yield
     for k in range(1, nz):
         for j in range(1, ns):
             copies.arrive(second[k, j])
@@ -105,43 +114,63 @@
             copies.start(piece, piece, partner)
 
 
-def ring_gather(copies, src, dst):
+def line_gather(copies, src, dst):
     nz = lax.axis_size("dp") // 2
     d = lax.axis_index("dp")
     z, c = d // 2, lax.rem(d, 2)
     partner = {"dp": d + 1 - 2 * c}
     up = {"dp": 2 * lax.rem(z + 1, nz) + c}
     down = {"dp": 2 * lax.rem(z + nz - 1, nz) + c}
-    a = copies.start(src.at[0], dst.at[d, 0], up)
-    b = copies.start(src.at[1], dst.at[d, 1], down)
+    below, above = {}, {}
+
+    def send(k):
+        low, high = 2 * lax.rem(z + nz - k, nz) + c, 2 * lax.rem(z + k, nz) + c
+        low_src, high_src = (dst.at[low], dst.at[high]) if k else (src, src)
+        below[k] = copies.start(
+            low_src, dst.at[low], up, jnp.logical_and(z >= k, z < nz - 1), z >= k + 1
+        )
+        above[k] = copies.start(
+            high_src, dst.at[high], down, jnp.logical_and(z + k < nz, z > 0), z + k + 1 < nz
+        )
+
+    send(0)
+    yield
     copies.keep(src, dst.at[d])
     copies.start(src, dst.at[d], partner)
     for k in range(1, nz):
-        low = dst.at[2 * lax.rem(z + nz - k, nz) + c, 0]
-        high = dst.at[2 * lax.rem(z + k, nz) + c, 1]
-        copies.arrive(a)
+        copies.arrive(below[k - 1])
+        copies.arrive(above[k - 1])
         if k < nz - 1:
-            a = copies.start(low, low, up)
-        copies.arrive(b)
-        if k < nz - 1:
-            b = copies.start(high, high, down)
-        copies.start(low, low, partner)
-        copies.start(high, high, partner)
+            send(k)
+        low, high = dst.at[2 * lax.rem(z + nz - k, nz) + c], dst.at[2 * lax.rem(z + k, nz) + c]
+        copies.start(low, low, partner, z >= k, z >= k)
+        copies.start(high, high, partner, z + k < nz, z + k < nz)
+        yield
 
 
 def run(axes, items, *refs):
     n = len(items)
     copies = Copies(*refs[2 * n :])
     greet(axes)
+    waiting = []
     for i, (kind, axis) in enumerate(items):
         src, dst = refs[i], refs[n + i]
         if kind == "spread":
-            spread_gather(copies, src, dst)
-        elif kind == "ring":
-            ring_gather(copies, src, dst)
+            waiting.append(spread_gather(copies, src, dst))
+        elif kind == "line":
+            waiting.append(line_gather(copies, src, dst))
+        elif kind == "later":
+            waiting.append(later(copies, axis, src, dst))
         else:
             direct(copies, kind, axis, src, dst)
+    while waiting:
+        waiting = [steps for steps in waiting if next(steps, waiting) is None]
     copies.finish()
+
+
+def later(copies, axis, src, dst):
+    yield
+    direct(copies, "scatter", axis, src, dst)
 
 
 def exchange(collective_id, *items):
@@ -152,7 +181,7 @@
         if kind in ("next", "prev"):
             shape = x.shape
             remote += 1
-        elif kind == "scatter":
+        elif kind in ("scatter", "later"):
             shape = x.shape
             remote += n - 1
             local += 1
@@ -201,17 +230,9 @@
 
     tail = (value[length - edge :] * jax.nn.sigmoid(gate[length - edge :])).astype(jnp.bfloat16)
     up_blocks = jnp.swapaxes(up.reshape(length, ndp, rows), 0, 1)
-    before, taps, up_columns, weight = exchange(
-        1,
-        ("next", "sp", tail),
-        ("gather", "sp", conv_taps),
-        ("scatter", "dp", up_blocks),
-        ("spread", "dp", out_weight.reshape(nsp, rows // nsp, channels)),
-    )
+    before, taps = exchange(1, ("next", "sp", tail), ("gather", "sp", conv_taps))
     before = jnp.where(at_start, 0, before)[edge - halo :]
     taps = jnp.swapaxes(taps, 0, 1).reshape(tap_count, channels)
-    up_columns = up_columns.reshape(ndp * length, rows)
-    weight = weight.reshape(ndp * rows, channels)
     sig_gate = jax.nn.sigmoid(gate)
     glu = (value * sig_gate).astype(jnp.bfloat16)
     padded = jnp.concatenate([before, glu], axis=0).astype(f32)
@@ -227,6 +248,19 @@
     sig = jax.nn.sigmoid(scaled)
     activated = (scaled * sig).astype(jnp.bfloat16)
 
+    weight, act_all, up_columns = exchange(
+        2,
+        ("spread", "dp", out_weight.reshape(nsp, rows // nsp, channels)),
+        ("line", "dp", activated),
+        ("later", "dp", up_blocks),
+    )
+    weight = weight.reshape(ndp * rows, channels)
+    act_all = act_all.reshape(ndp * length, channels)
+    up_columns = up_columns.reshape(ndp * length, rows)
+    owned = lax.dot_general(
+        up_columns, act_all, (((0,), (0,)), ((), ())), preferred_element_type=f32
+    )
+
     grad_act = jnp.dot(up, weight, preferred_element_type=f32)
     grad_scaled = grad_act * sig * (1.0 + scaled * (1.0 - sig))
     gain_part = jnp.sum(grad_scaled * normed, axis=0)
@@ -237,13 +271,13 @@
         - normed * jnp.mean(g * normed, axis=-1, keepdims=True)
     )
     grad_conv = grad_conv.astype(jnp.bfloat16)
-    after, act_all = exchange(
-        2,
+    after, gain_got, owned_got = exchange(
+        3,
         ("prev", "sp", grad_conv[:edge]),
-        ("ring", "dp", activated.reshape(2, length // 2, channels)),
+        ("gather", "sp", gain_part[None]),
+        ("scatter", "sp", owned.astype(jnp.bfloat16).reshape(nsp, rows // nsp, channels)),
     )
     after = jnp.where(at_end, 0, after)[:halo]
-    act_all = act_all.reshape(ndp * length, channels)
     extended = jnp.concatenate([grad_conv, after], axis=0).astype(f32)
     here = grad_conv.astype(f32)
     grad_glu = jnp.zeros_like(here)
@@ -256,23 +290,15 @@
     grad_value = (grad_glu * sig_gate).astype(jnp.bfloat16)
     grad_gate = (grad_glu * value * sig_gate * (1.0 - sig_gate)).astype(jnp.bfloat16)
 
-    owned = lax.dot_general(
-        up_columns, act_all, (((0,), (0,)), ((), ())), preferred_element_type=f32
-    )
     width = conv_taps.shape[1]
     tap_blocks = jnp.swapaxes(jnp.stack(terms).reshape(tap_count, nsp, width), 0, 1)
-    gain_got, tap_got, owned_got = exchange(
-        3,
-        ("gather", "sp", gain_part[None]),
-        ("scatter", "sp", tap_blocks),
-        ("scatter", "sp", owned.astype(jnp.bfloat16).reshape(nsp, rows // nsp, channels)),
-    )
     gain_got, tap_got, grad_weight = exchange(
         4,
         ("gather", "dp", jnp.sum(gain_got, axis=0)),
-        ("gather", "dp", jnp.sum(tap_got, axis=0)),
+        ("scatter", "sp", tap_blocks),
         ("gather", "sp", jnp.sum(owned_got.astype(f32), axis=0).astype(jnp.bfloat16)),
     )
+    (tap_got,) = exchange(5, ("gather", "dp", jnp.sum(tap_got, axis=0)))
     grad_gain = jnp.sum(gain_got, axis=0)[0]
     grad_taps = jnp.sum(tap_got, axis=0)
     grad_weight = grad_weight.reshape(rows, channels).astype(f32)

time: 261 us -> 247 us (0.946)
  Pallas kernels: 199 us -> 187 us
  local copies, waits for them, and re-layouts: 9.86 us -> 6.08 us
    pallas_call x4 -> x5, Pallas kernels: 199 us -> 187 us  [exchange(): pl.pallas_call(functools.partial(run, axes, tuple(((kind, axis) for kind,...]
    another operation x1, local copies, waits for them, and re-layouts: 3.63 us -> 0.43 us  [body(): jnp.stack(terms).reshape(tap_count, nsp, width)]
where the time goes in v3:
time: 247 us; the launch traced here: 246 us
  Pallas kernels  187 us (76%)
  other arithmetic  39.9 us (16%)
  matrix products  11.6 us (5%)
  local copies, waits for them, and re-layouts  6.08 us (2%)
    pallas_call x5, Pallas kernels, exchange(): pl.pallas_call(functools.partial(run, axes, tuple(((kind, axis) for kind,...  187 us
    reduce_sum x1, other arithmetic, body(): mean = jnp.mean(conv, axis=-1, keepdims=True)  10.9 us
    reduce_sum x2, other arithmetic, body(): terms.append(jnp.sum(here * padded[j:j + length], axis=0))  10.3 us
    broadcast_in_dim x1, other arithmetic, body(): grad_gate[None]  9.49 us
    dot_general x1, matrix products, body(): grad_act = jnp.dot(up, weight, preferred_element_type=f32)  5.84 us
    dot_general x1, matrix products, body(): lax.dot_general(up_columns, act_all, (((0,), (0,)), ((), ())), preferred_...  5.72 us

profile of v3, /device:TPU:0, one launch (start us, length us, event | category | flops | bytes accessed | tf_op | source)
XLA Modules:
  0.0 245.8 jit_solution(12056555540097065106)
XLA Ops:
  0.6 0.0 copy-start.2
  0.6 0.0 copy-start.4
  0.7 2.4 copy.12
  3.1 1.5 copy.13
  4.6 0.6 fusion.89
  5.1 0.2 convert_element_type.63
  5.4 0.0 copy-start.1
  5.4 0.2 convert_element_type.64
  5.6 0.1 fusion.98.refs_0_
  5.7 0.5 copy-done.1
  6.2 10.6 %shard_map.101 = (bf16[32,2048]{1,0:T(8,128)(2,1)S(1)}, f32[4,31,512]{2,1,0:T(8,128)S(1)}) custom-call(bf16[32,2048]{1,0:T(8,128)(2,1)S(1)} %fusion.98.refs_0_, f32[31,512]{1,0:T(8,128)S(1)} %copy-done.1), custom_call_target="tpu_custom_call" | custom-call | tf_op jit(solution)/shard_map/pallas_call | solution.py:199
  16.9 0.1 fusion.102
  16.9 0.1 fusion.101
  17.1 0.0 copy-start.7
  17.1 0.0 copy-start.9
  17.2 0.3 maximum_convert_fusion
  17.6 0.0 copy-start.33
  17.6 10.9 %convert_reduce_fusion = (f32[256]{0:T(256)S(1)}, bf16[256,2048]{1,0:T(8,128)(2,1)S(1)}) fusion(f32[286,2048]{1,0:T(8,128)S(1)} %maximum_convert_fusion, f32[2048]{0:T(1024)S(1)} %bitcast.151, f32[2048]{0:T(1024)S(1)} %bitcast.153, f32[2048]{0:T(1024)S(1)} %bitcast.155, f32[2048]{0:T(1024)S(1)} %bitcast.157, f32[2048]{0:T(1024)S(1)} %bitcast.159, ...), kind=kLoop, calls=%fused_computation.38 | loop fusion | flops 33554176 | bytes 66315264 | tf_op jit(solution)/shard_map/reduce_sum | solution.py:243
  28.5 0.0 copy-done.7
  28.5 0.0 copy-done.9
  28.5 0.0 copy-done.11
  28.6 0.0 copy-done.13
  28.6 0.0 copy-done.15
  28.6 0.0 copy-done.17
  28.7 0.0 copy-start
  28.7 0.4 fusion.22
  29.1 0.9 fusion.15.refs_1_
  30.0 0.0 copy-start.6
  30.0 127.6 %shard_map.102 = (bf16[8,4,64,2048]{3,2,1,0:T(8,128)(2,1)}, bf16[8,256,2048]{2,1,0:T(8,128)(2,1)}, bf16[8,256,256]{2,1,0:T(8,128)(2,1)S(1)}) custom-call(bf16[4,64,2048]{2,1,0:T(8,128)(2,1)S(1)} %bitcast.118, bf16[256,2048]{1,0:T(8,128)(2,1)S(1)} %fusion.15.refs_1_, bf16[8,256,256]{2,1,0:T(8,128)(2,1)S(1)} %bitcast.116), custom_call_target="tpu_custom_call" | custom-call | tf_op jit(solution)/shard_map/pallas_call | solution.py:199
  157.6 5.8 %fusion.21 = (f32[2048]{0:T(1024)S(1)}, f32[256]{0:T(256)S(1)}, f32[256]{0:T(256)S(1)}, f32[256,2048]{1,0:T(8,128)S(1)}) fusion(bf16[256,2048]{1,0:T(8,128)(2,1)S(1)} %get-tuple-element.65, f32[256]{0:T(256)S(1)} %add_rsqrt_fusion, f32[256]{0:T(256)S(1)} %broadcast_multiply_fusion.2, f32[2048]{0:T(1024)S(1)} %copy-done.33, ...), kind=kOutput, calls=%fused_computation.58 | convolution fusion | flops 2156918272 | bytes 12603392 | tf_op jit(solution)/shard_map/dot_general | solution.py:264
  163.5 6.6 %fusion.57 = (f32[2048]{0:T(1024)S(1)}, f32[2048]{0:T(1024)S(1)}, f32[2048]{0:T(1024)S(1)}, f32[2048]{0:T(1024)S(1)}, f32[2048]{0:T(1024)S(1)}, /*index=5*/f32[2...) fusion(f32[286,2048]{1,0:T(8,128)S(1)} %maximum_convert_fusion,, ...), kind=kLoop, calls=%fused_computation.94 | loop fusion | flops 24080384 | bytes 42102784 | tf_op jit(solution)/shard_map/reduce_sum | solution.py:288
  170.1 0.0 copy-start.3
  170.1 3.7 %fusion.56 = (f32[2048]{0:T(1024)S(1)}, f32[2048]{0:T(1024)S(1)}, f32[2048]{0:T(1024)S(1)}, f32[2048]{0:T(1024)S(1)}, f32[2048]{0:T(1024)S(1)}, /*index=5*/f32[2...) fusion(bf16[256,2048]{1,0:T(8,128)(2,1)S(1)} %get-tuple-element, ...), kind=kLoop, calls=%fused_computation.93 | loop fusion | flops 14129152 | bytes 28418048 | tf_op jit(solution)/shard_map/reduce_sum | solution.py:288
  173.8 0.4 stack.127
  174.3 0.9 slice.555.refs_0_
  175.2 5.7 %fusion.2 = bf16[256,2048]{1,0:T(8,128)(2,1)S(1)} fusion(bf16[8,256,256]{2,1,0:T(8,128)(2,1)S(1)} %get-tuple-element.19, bf16[8,256,2048]{2,1,0:T(8,128)(2,1)} %get-tuple-element.20), kind=kOutput, calls=%fused_computation.39 | convolution fusion | flops 2148007936 | bytes 10485760 | tf_op jit(solution)/shard_map/dot_general | solution.py:260
  180.9 18.7 %shard_map.103 = (bf16[32,2048]{1,0:T(8,128)(2,1)S(1)}, f32[4,1,2048]{2,1,0:T(1,128)S(1)}, bf16[4,64,2048]{2,1,0:T(8,128)(2,1)S(1)}) custom-call(bf16[32,2048]{1,0:T(8,128)(2,1)S(1)} %slice.555.refs_0_, f32[1,2048]{1,0:T(1,128)S(1)} %bitcast.123, bf16[4,64,2048]{2,1,0:T(8,128)(2,1)S(1)} %bitcast.117), custom_call_target="tpu_custom_call" | custom-call | tf_op jit(solution)/shard_map/pallas_call | solution.py:199
  199.7 0.2 reduce_sum.412.refs_2_
  199.9 17.5 %shard_map.104 = (f32[8,1,2048]{2,1,0:T(1,128)S(1)}, f32[4,31,512]{2,1,0:T(8,128)S(1)}, bf16[4,64,2048]{2,1,0:T(8,128)(2,1)S(1)}) custom-call(f32[1,2048]{1,0:T(1,128)S(1)} %bitcast.122, f32[4,31,512]{2,1,0:T(8,128)S(1)} %bitcast.119, bf16[64,2048]{1,0:T(8,128)(2,1)S(1)} %reduce_sum.412.refs_2_), custom_call_target="tpu_custom_call" | custom-call | tf_op jit(solution)/shard_map/pallas_call | solution.py:199
  217.5 0.7 reduce_sum.415
  218.1 12.5 %shard_map.105 = f32[8,31,512]{2,1,0:T(8,128)S(1)} custom-call(f32[31,512]{1,0:T(8,128)S(1)} %reduce_sum.413.refs_0_), custom_call_target="tpu_custom_call" | custom-call | tf_op jit(solution)/shard_map/pallas_call | solution.py:199
  230.6 0.0 copy-start.8
  230.6 0.0 copy-start.10
  230.7 0.7 reduce_sum.414
  231.4 1.6 maximum_convert_fusion.1
  233.1 9.5 %fusion.90 = (bf16[1,256,2048]{2,1,0:T(8,128)(2,1)}, bf16[256,2048]{1,0:T(8,128)(2,1)S(1)}) fusion(bf16[1,256,2048]{2,1,0:T(8,128)(2,1)S(1)} %copy-done.5, bf16[1,256,2048]{2,1,0:T(8,128)(2,1)S(1)} %copy-done.2, f32[286,2048]{1,0:T(8,128)S(1)} %maximum_convert_fusion.1, f32[2048]{0:T(1024)S(1)} %bitcast.152, f32[2048]{0:T(1024)S(1)} %bitcast.154, ...), kind=kLoop, calls=%fused_computation.165 | loop fusion | flops 38273024 | bytes 69459968 | tf_op jit(solution)/shard_map/broadcast_in_dim | solution.py:305
  242.6 1.6 fusion.91
  244.1 1.6 bitcast_convert_fusion
  (57 shorter events, 0.2 us)
Async XLA Ops:
  0.6 3.9 %copy-start.2 = (bf16[1,256,2048]{2,1,0:T(8,128)(2,1)S(1)}, bf16[1,256,2048]{2,1,0:T(8,128)(2,1)}, u32[]{:S(2)}) copy-start(bf16[1,256,2048]{2,1,0:T(8,128)(2,1)} %param.7) | copy-start | bytes 3145732
  0.6 3.9 %copy-start.4 = (bf16[1,256,2048]{2,1,0:T(8,128)(2,1)S(1)}, bf16[1,256,2048]{2,1,0:T(8,128)(2,1)}, u32[]{:S(2)}) copy-start(bf16[1,256,2048]{2,1,0:T(8,128)(2,1)} %param.6) | copy-start | bytes 3145732
  5.4 0.8 copy-start.1
  17.1 11.5 %copy-start.7 = (f32[1,4,512]{2,0,1:T(1,128)}, f32[1,4,512]{2,0,1:T(1,128)S(1)}, u32[]{:S(2)}) copy-start(f32[1,4,512]{2,0,1:T(1,128)S(1)} %get-tuple-element.72) | copy-start | bytes 24580
  17.1 11.5 %copy-start.9 = (f32[1,4,512]{2,0,1:T(1,128)}, f32[1,4,512]{2,0,1:T(1,128)S(1)}, u32[]{:S(2)}) copy-start(f32[1,4,512]{2,0,1:T(1,128)S(1)} %get-tuple-element.73) | copy-start | bytes 24580
  17.1 11.5 %copy-start.11 = (f32[1,4,512]{2,0,1:T(1,128)}, f32[1,4,512]{2,0,1:T(1,128)S(1)}, u32[]{:S(2)}) copy-start(f32[1,4,512]{2,0,1:T(1,128)S(1)} %get-tuple-element.74) | copy-start | bytes 24580
  17.1 11.5 %copy-start.13 = (f32[1,4,512]{2,0,1:T(1,128)}, f32[1,4,512]{2,0,1:T(1,128)S(1)}, u32[]{:S(2)}) copy-start(f32[1,4,512]{2,0,1:T(1,128)S(1)} %get-tuple-element.75) | copy-start | bytes 24580
  17.1 11.5 %copy-start.15 = (f32[1,4,512]{2,0,1:T(1,128)}, f32[1,4,512]{2,0,1:T(1,128)S(1)}, u32[]{:S(2)}) copy-start(f32[1,4,512]{2,0,1:T(1,128)S(1)} %get-tuple-element.76) | copy-start | bytes 24580
  17.1 11.5 %copy-start.17 = (f32[1,4,512]{2,0,1:T(1,128)}, f32[1,4,512]{2,0,1:T(1,128)S(1)}, u32[]{:S(2)}) copy-start(f32[1,4,512]{2,0,1:T(1,128)S(1)} %get-tuple-element.77) | copy-start | bytes 24580
  17.1 11.5 %copy-start.19 = (f32[1,4,512]{2,0,1:T(1,128)}, f32[1,4,512]{2,0,1:T(1,128)S(1)}, u32[]{:S(2)}) copy-start(f32[1,4,512]{2,0,1:T(1,128)S(1)} %get-tuple-element.78) | copy-start | bytes 24580
  17.1 11.5 %copy-start.21 = (f32[1,4,512]{2,0,1:T(1,128)}, f32[1,4,512]{2,0,1:T(1,128)S(1)}, u32[]{:S(2)}) copy-start(f32[1,4,512]{2,0,1:T(1,128)S(1)} %get-tuple-element.79) | copy-start | bytes 24580
  17.1 11.5 %copy-start.23 = (f32[1,4,512]{2,0,1:T(1,128)}, f32[1,4,512]{2,0,1:T(1,128)S(1)}, u32[]{:S(2)}) copy-start(f32[1,4,512]{2,0,1:T(1,128)S(1)} %get-tuple-element.80) | copy-start | bytes 24580
  17.2 11.5 %copy-start.25 = (f32[1,4,512]{2,0,1:T(1,128)}, f32[1,4,512]{2,0,1:T(1,128)S(1)}, u32[]{:S(2)}) copy-start(f32[1,4,512]{2,0,1:T(1,128)S(1)} %get-tuple-element.81) | copy-start | bytes 24580
  17.2 11.5 %copy-start.27 = (f32[1,4,512]{2,0,1:T(1,128)}, f32[1,4,512]{2,0,1:T(1,128)S(1)}, u32[]{:S(2)}) copy-start(f32[1,4,512]{2,0,1:T(1,128)S(1)} %get-tuple-element.82) | copy-start | bytes 24580
  17.2 11.5 %copy-start.29 = (f32[1,4,512]{2,0,1:T(1,128)}, f32[1,4,512]{2,0,1:T(1,128)S(1)}, u32[]{:S(2)}) copy-start(f32[1,4,512]{2,0,1:T(1,128)S(1)} %get-tuple-element.83) | copy-start | bytes 24580
  17.2 11.5 %copy-start.31 = (f32[1,4,512]{2,0,1:T(1,128)}, f32[1,4,512]{2,0,1:T(1,128)S(1)}, u32[]{:S(2)}) copy-start(f32[1,4,512]{2,0,1:T(1,128)S(1)} %get-tuple-element.84) | copy-start | bytes 24580
  17.6 11.5 %copy-start.33 = (f32[2048]{0:T(1024)S(1)}, f32[2048]{0:T(1024)}, u32[]{:S(2)}) copy-start(f32[2048]{0:T(1024)} %param.10) | copy-start | bytes 24580
  28.7 1.3 copy-start
  30.0 127.6 %copy-start.6 = (bf16[1,256,2048]{2,1,0:T(8,128)(2,1)S(1)}, bf16[1,256,2048]{2,1,0:T(8,128)(2,1)}, u32[]{:S(2)}) copy-start(bf16[1,256,2048]{2,1,0:T(8,128)(2,1)} %param.8) | copy-start | bytes 3145732
  170.1 3.8 %copy-start.3 = (bf16[256,2048]{1,0:T(8,128)(2,1)}, bf16[256,2048]{1,0:T(8,128)(2,1)S(1)}, u32[]{:S(2)}) copy-start(bf16[256,2048]{1,0:T(8,128)(2,1)S(1)} %get-tuple-element.61) | copy-start | bytes 3145732
  230.6 2.4 copy-start.8
  230.6 2.4 copy-start.10
  230.6 2.4 copy-start.12
  230.6 2.4 copy-start.14
  230.6 2.4 copy-start.16
  230.6 2.4 copy-start.18
  230.6 2.4 copy-start.20
  230.7 2.4 copy-start.22
  230.7 2.4 copy-start.24
  230.7 2.4 copy-start.26
  230.7 2.4 copy-start.28
  230.7 2.4 copy-start.30
  230.7 2.4 copy-start.32
  231.4 1.7 copy-start.5

commit v4 on v3

--- a/solution.py
+++ b/solution.py
@@ -80,6 +80,16 @@
     me = lax.axis_index(axis)
     if kind == "next" or kind == "prev":
         copies.start(src, dst, {axis: lax.rem(me + (1 if kind == "next" else n - 1), n)})
+        return
+    if kind == "pair":
+        copies.start(src, dst, {axis: me + 1 - 2 * lax.rem(me, 2)})
+        return
+    if kind == "rows":
+        nz, z, c = n // 2, me // 2, lax.rem(me, 2)
+        copies.keep(src.at[z], dst.at[z])
+        for k in range(1, nz):
+            peer = lax.rem(z + k, nz)
+            copies.start(src.at[peer], dst.at[z], {axis: 2 * peer + c})
         return
     copies.keep(src.at[me] if kind == "scatter" else src, dst.at[me])
     for k in range(1, n):
@@ -178,7 +188,11 @@
     shapes, remote, local = [], 0, 0
     for kind, axis, x in items:
         n = lax.axis_size(axis)
-        if kind in ("next", "prev"):
+        if kind == "rows":
+            shape = x.shape
+            remote += n // 2 - 1
+            local += 1
+        elif kind in ("next", "prev", "pair"):
             shape = x.shape
             remote += 1
         elif kind in ("scatter", "later"):
@@ -248,18 +262,33 @@
     sig = jax.nn.sigmoid(scaled)
     activated = (scaled * sig).astype(jnp.bfloat16)
 
-    weight, act_all, up_columns = exchange(
+    half = channels // 2
+    nz, piece = ndp // 2, rows // nsp
+    core = lax.rem(lax.axis_index("dp"), 2)
+    by_core = up.reshape(length, nz, 2, nsp, piece)
+
+    def partial(which):
+        columns = lax.dynamic_index_in_dim(by_core, which, 2, keepdims=False)
+        columns = jnp.swapaxes(columns, 1, 2).reshape(length, nsp * nz * piece)
+        return lax.dot_general(
+            columns, activated[:, half:], (((0,), (0,)), ((), ())), preferred_element_type=f32
+        )
+
+    weight, act_all, up_columns, from_partner = exchange(
         2,
         ("spread", "dp", out_weight.reshape(nsp, rows // nsp, channels)),
-        ("line", "dp", activated),
+        ("line", "dp", activated[:, :half]),
         ("later", "dp", up_blocks),
+        ("pair", "dp", partial(1 - core).astype(jnp.bfloat16)),
     )
     weight = weight.reshape(ndp * rows, channels)
-    act_all = act_all.reshape(ndp * length, channels)
+    act_all = act_all.reshape(ndp * length, half)
     up_columns = up_columns.reshape(ndp * length, rows)
     owned = lax.dot_general(
         up_columns, act_all, (((0,), (0,)), ((), ())), preferred_element_type=f32
     )
+    summed = (partial(core) + from_partner.astype(f32)).astype(jnp.bfloat16)
+    summed = summed.reshape(nsp, nz, piece, half)
 
     grad_act = jnp.dot(up, weight, preferred_element_type=f32)
     grad_scaled = grad_act * sig * (1.0 + scaled * (1.0 - sig))
@@ -271,11 +300,12 @@
         - normed * jnp.mean(g * normed, axis=-1, keepdims=True)
     )
     grad_conv = grad_conv.astype(jnp.bfloat16)
-    after, gain_got, owned_got = exchange(
+    after, gain_got, owned_got, summed_got = exchange(
         3,
         ("prev", "sp", grad_conv[:edge]),
         ("gather", "sp", gain_part[None]),
-        ("scatter", "sp", owned.astype(jnp.bfloat16).reshape(nsp, rows // nsp, channels)),
+        ("scatter", "sp", owned.astype(jnp.bfloat16).reshape(nsp, piece, half)),
+        ("scatter", "sp", summed),
     )
     after = jnp.where(at_end, 0, after)[:halo]
     extended = jnp.concatenate([grad_conv, after], axis=0).astype(f32)
@@ -292,16 +322,23 @@
 
     width = conv_taps.shape[1]
     tap_blocks = jnp.swapaxes(jnp.stack(terms).reshape(tap_count, nsp, width), 0, 1)
-    gain_got, tap_got, grad_weight = exchange(
+    gain_got, tap_got, low_weight, high_got = exchange(
         4,
         ("gather", "dp", jnp.sum(gain_got, axis=0)),
         ("scatter", "sp", tap_blocks),
         ("gather", "sp", jnp.sum(owned_got.astype(f32), axis=0).astype(jnp.bfloat16)),
-    )
-    (tap_got,) = exchange(5, ("gather", "dp", jnp.sum(tap_got, axis=0)))
+        ("rows", "dp", jnp.sum(summed_got.astype(f32), axis=0).astype(jnp.bfloat16)),
+    )
+    tap_got, high_weight = exchange(
+        5,
+        ("gather", "dp", jnp.sum(tap_got, axis=0)),
+        ("gather", "sp", jnp.sum(high_got.astype(f32), axis=0).astype(jnp.bfloat16)),
+    )
     grad_gain = jnp.sum(gain_got, axis=0)[0]
     grad_taps = jnp.sum(tap_got, axis=0)
-    grad_weight = grad_weight.reshape(rows, channels).astype(f32)
+    grad_weight = jnp.concatenate(
+        [low_weight.reshape(rows, half), high_weight.reshape(rows, half)], axis=1
+    ).astype(f32)
     return (grad_value[None], grad_gate[None], grad_taps, grad_gain, grad_weight)
 
 

time: 247 us -> 237 us (0.960)
  Pallas kernels: 187 us -> 168 us
  local copies, waits for them, and re-layouts: 6.08 us -> 13.1 us
    pallas_call x5, Pallas kernels: 187 us -> 168 us  [exchange(): pl.pallas_call(functools.partial(run, axes, tuple(((kind, axis) for kind,...]
    another operation x1, local copies, waits for them, and re-layouts: 0.43 us -> 3.63 us  [body(): jnp.stack(terms).reshape(tap_count, nsp, width)]
    dot_general x0 -> x2, matrix products: none -> 2.75 us  [partial(): lax.dot_general(columns, activated[:, half:], (((0,), (0,)), ((), ())), p...]
    unnamed x69 -> x91, local copies, waits for them, and re-layouts: 3.07 us -> 5.14 us
where the time goes in v4:
time: 237 us; the launch traced here: 235 us
  Pallas kernels  168 us (71%)
  other arithmetic  40.2 us (17%)
  local copies, waits for them, and re-layouts  13.1 us (6%)
  matrix products  12.5 us (5%)
    pallas_call x5, Pallas kernels, exchange(): pl.pallas_call(functools.partial(run, axes, tuple(((kind, axis) for kind,...  168 us
    reduce_sum x2, other arithmetic, body(): terms.append(jnp.sum(here * padded[j:j + length], axis=0))  11.6 us
    reduce_sum x1, other arithmetic, body(): mean = jnp.mean(conv, axis=-1, keepdims=True)  11 us
    broadcast_in_dim x1, other arithmetic, body(): grad_gate[None]  9.5 us
    dot_general x1, matrix products, body(): grad_act = jnp.dot(up, weight, preferred_element_type=f32)  6.21 us
    unnamed x91, local copies, waits for them, and re-layouts  5.14 us

profile of v4, /device:TPU:0, one launch (start us, length us, event | category | flops | bytes accessed | tf_op | source)
XLA Modules:
  0.0 235.1 jit_solution(403880889660721539)
XLA Ops:
  0.6 1.5 copy.16
  2.1 0.0 copy-start.10
  2.1 0.1 dynamic-slice_bitcast_fusion
  2.3 0.8 copy-done.10
  3.1 0.8 copy.21
  3.9 0.8 copy.19
  4.8 1.5 copy.17
  6.3 0.6 fusion.88
  6.8 0.2 convert_element_type.73
  7.1 0.0 copy-start.1
  7.1 0.2 convert_element_type.74
  7.3 0.1 fusion.100.refs_0_
  7.4 0.5 copy-done.1
  7.9 10.6 %shard_map.101 = (bf16[32,2048]{1,0:T(8,128)(2,1)S(1)}, f32[4,31,512]{2,1,0:T(8,128)S(1)}) custom-call(bf16[32,2048]{1,0:T(8,128)(2,1)S(1)} %fusion.100.refs_0_, f32[31,512]{1,0:T(8,128)S(1)} %copy-done.1), custom_call_target="tpu_custom_call" | custom-call | tf_op jit(solution)/shard_map/pallas_call | solution.py:213
  18.5 0.1 fusion.104
  18.6 0.1 fusion.103
  18.9 0.3 maximum_convert_fusion
  19.3 11.0 %convert_reduce_fusion = (f32[256]{0:T(256)S(1)}, bf16[256,2048]{1,0:T(8,128)(2,1)S(1)}) fusion(f32[286,2048]{1,0:T(8,128)S(1)} %maximum_convert_fusion, f32[2048]{0:T(1024)S(1)} %bitcast.170, f32[2048]{0:T(1024)S(1)} %bitcast.172, f32[2048]{0:T(1024)S(1)} %bitcast.174, f32[2048]{0:T(1024)S(1)} %bitcast.176, f32[2048]{0:T(1024)S(1)} %bitcast.178, ...), kind=kLoop, calls=%fused_computation.38 | loop fusion | flops 33554176 | bytes 66315264 | tf_op jit(solution)/shard_map/reduce_sum | solution.py:257
  30.4 0.0 copy-start.14
  30.4 0.4 fusion.21
  30.8 0.9 fusion.14
  31.7 0.0 copy-start
  31.8 1.0 copy-done.11
  32.8 2.0 convolution_convert_fusion.refs_3_
  34.8 93.5 %shard_map.102 = (bf16[8,4,64,2048]{3,2,1,0:T(8,128)(2,1)}, bf16[8,256,1024]{2,1,0:T(8,128)(2,1)}, bf16[8,256,256]{2,1,0:T(8,128)(2,1)S(1)}, bf16[1024,1024]{1,0:T(8,128)(2,1)S(1)}) custom-call(bf16[4,64,2048]{2,1,0:T(8,128)(2,1)S(1)} %bitcast.132, bf16[256,1024]{1,0:T(8,128)(2,1)S(1)} %slice.564.refs_1_, bf16[8,256,256]{2,1,0:T(8,128)(2,1)S(1)} %bitcast.130, ...), custom_call_target="tpu_custom_call" | custom-call | tf_op jit(solution)/shard_map/pallas_call | solution.py:213
  128.3 0.0 copy-start.2
  128.3 6.2 %fusion.20 = (f32[2048]{0:T(1024)S(1)}, f32[256]{0:T(256)S(1)}, f32[256]{0:T(256)S(1)}, f32[256,2048]{1,0:T(8,128)S(1)}) fusion(bf16[256,2048]{1,0:T(8,128)(2,1)S(1)} %get-tuple-element.75, f32[256]{0:T(256)S(1)} %add_rsqrt_fusion, f32[256]{0:T(256)S(1)} %broadcast_multiply_fusion.2, f32[2048]{0:T(1024)S(1)} %copy-done.44, ...), kind=kOutput, calls=%fused_computation.57 | convolution fusion | flops 2156918272 | bytes 12603392 | tf_op jit(solution)/shard_map/dot_general | solution.py:293
  134.5 7.2 %fusion.56 = (f32[2048]{0:T(1024)}, f32[2048]{0:T(1024)}, f32[2048]{0:T(1024)}, f32[2048]{0:T(1024)}, f32[2048]{0:T(1024)}, /*index=5*/f32[2048]{0:T(1024)}, f32...) fusion(f32[286,2048]{1,0:T(8,128)S(1)} %maximum_convert_fusion,, ...), kind=kLoop, calls=%fused_computation.93 | loop fusion | flops 24080384 | bytes 42102784 | tf_op jit(solution)/shard_map/reduce_sum | solution.py:318
  141.7 4.4 %fusion.55 = (f32[2048]{0:T(1024)}, f32[2048]{0:T(1024)}, f32[2048]{0:T(1024)}, f32[2048]{0:T(1024)}, f32[2048]{0:T(1024)}, /*index=5*/f32[2048]{0:T(1024)}, f32...) fusion(bf16[256,2048]{1,0:T(8,128)(2,1)S(1)} %get-tuple-element, ...), kind=kLoop, calls=%fused_computation.92 | loop fusion | flops 14129152 | bytes 28418048 | tf_op jit(solution)/shard_map/reduce_sum | solution.py:318
  146.1 3.6 %stack.127 = f32[31,4,512]{2,0,1:T(8,128)S(1)} concatenate(f32[1,4,512]{2,0,1:T(1,128)} %bitcast.218, f32[1,4,512]{2,0,1:T(1,128)} %bitcast.220, f32[1,4,512]{2,0,1:T(1,128)} %bitcast.221, f32[1,4,512]{2,0,1:T(1,128)} %bitcast.222, f32[1,4,512]{2,0,1:T(1,128)} %bitcast.223, f32[1,4,512]{2,0,1:T(1,128)} %bitcast.224, f32[1,4,512]{2,0,1:T(1,128)} %bitcast.225, ...), dimensions={0} | concatenate | bytes 507904 | tf_op jit(solution)/shard_map/stack | solution.py:324
  149.8 0.9 slice.566.refs_0_
  150.7 3.6 %fusion.89 = bf16[256,1024]{1,0:T(8,128)(2,1)S(1)} fusion(bf16[8,256,256]{2,1,0:T(8,128)(2,1)S(1)} %copy-done.3, bf16[8,256,1024]{2,1,0:T(8,128)(2,1)} %get-tuple-element.25), kind=kOutput, calls=%fused_computation.164 | convolution fusion | flops 1074003968 | bytes 5767168 | tf_op jit(solution)/shard_map/dot_general | solution.py:287
  154.3 0.7 add_convert_fusion
  155.0 35.8 %shard_map.103 = (bf16[32,2048]{1,0:T(8,128)(2,1)S(1)}, f32[4,1,2048]{2,1,0:T(1,128)S(1)}, bf16[4,64,1024]{2,1,0:T(8,128)(2,1)S(1)}, bf16[4,4,64,1024]{3,2,1,0:T(8,128)(2,1)S(1)}) custom-call(bf16[32,2048]{1,0:T(8,128)(2,1)S(1)} %slice.566.refs_0_, f32[1,2048]{1,0:T(1,128)S(1)} %bitcast.139, bf16[4,64,1024]{2,1,0:T(8,128)(2,1)S(1)} %bitcast.134, ...), custom_call_target="tpu_custom_call" | custom-call | tf_op jit(solution)/shard_map/pallas_call | solution.py:213
  190.9 0.1 reduce_sum.436.refs_2_
  191.0 0.4 reduce_sum.437.refs_3_
  191.4 14.7 %shard_map.104 = (f32[8,1,2048]{2,1,0:T(1,128)S(1)}, f32[4,31,512]{2,1,0:T(8,128)S(1)}, bf16[4,64,1024]{2,1,0:T(8,128)(2,1)S(1)}, bf16[4,64,1024]{2,1,0:T(8,128)(2,1)S(1)}) custom-call(f32[1,2048]{1,0:T(1,128)S(1)} %bitcast.138, f32[4,31,512]{2,1,0:T(8,128)S(1)} %bitcast.131, bf16[64,1024]{1,0:T(8,128)(2,1)S(1)} %reduce_sum.436.refs_2_, ...), custom_call_target="tpu_custom_call" | custom-call | tf_op jit(solution)/shard_map/pallas_call | solution.py:213
  206.2 0.7 reduce_sum.441
  206.8 0.1 reduce_sum.439.refs_1_
  206.9 0.0 copy-start.7
  206.9 13.2 %shard_map.105 = (f32[8,31,512]{2,1,0:T(8,128)S(1)}, bf16[4,64,1024]{2,1,0:T(8,128)(2,1)S(1)}) custom-call(f32[31,512]{1,0:T(8,128)S(1)} %reduce_sum.438.refs_0_, bf16[64,1024]{1,0:T(8,128)(2,1)S(1)} %reduce_sum.439.refs_1_), custom_call_target="tpu_custom_call" | custom-call | tf_op jit(solution)/shard_map/pallas_call | solution.py:213
  220.2 0.7 reduce_sum.440
  220.9 1.6 maximum_convert_fusion.2
  222.6 0.3 maximum_convert_fusion.1
  222.8 0.8 copy-done.5
  223.7 0.3 copy-done.9
  224.1 9.5 %fusion.90 = (bf16[1,256,2048]{2,1,0:T(8,128)(2,1)}, bf16[256,2048]{1,0:T(8,128)(2,1)S(1)}) fusion(bf16[1,256,2048]{2,1,0:T(8,128)(2,1)S(1)} %copy-done.9, bf16[1,256,2048]{2,1,0:T(8,128)(2,1)S(1)} %copy-done.5, f32[286,2048]{1,0:T(8,128)S(1)} %maximum_convert_fusion.1, f32[2048]{0:T(1024)S(1)} %bitcast.171, f32[2048]{0:T(1024)S(1)} %bitcast.173, ...), kind=kLoop, calls=%fused_computation.167 | loop fusion | flops 38273024 | bytes 69459968 | tf_op jit(solution)/shard_map/broadcast_in_dim | solution.py:342
  233.6 1.6 fusion.91
  (87 shorter events, 0.3 us)
Async XLA Ops:
  2.1 1.0 copy-start.10
  3.1 3.1 %copy-start.4 = (bf16[1,256,2048]{2,1,0:T(8,128)(2,1)S(1)}, bf16[1,256,2048]{2,1,0:T(8,128)(2,1)}, u32[]{:S(2)}) copy-start(bf16[1,256,2048]{2,1,0:T(8,128)(2,1)} %param.7) | copy-start | bytes 3145732
  3.1 3.1 %copy-start.8 = (bf16[1,256,2048]{2,1,0:T(8,128)(2,1)S(1)}, bf16[1,256,2048]{2,1,0:T(8,128)(2,1)}, u32[]{:S(2)}) copy-start(bf16[1,256,2048]{2,1,0:T(8,128)(2,1)} %param.6) | copy-start | bytes 3145732
  7.1 0.8 copy-start.1
  18.7 11.5 %copy-start.16 = (f32[1,4,512]{2,0,1:T(1,128)}, f32[1,4,512]{2,0,1:T(1,128)S(1)}, u32[]{:S(2)}) copy-start(f32[1,4,512]{2,0,1:T(1,128)S(1)} %get-tuple-element.83) | copy-start | bytes 24580
  18.8 11.5 %copy-start.18 = (f32[1,4,512]{2,0,1:T(1,128)}, f32[1,4,512]{2,0,1:T(1,128)S(1)}, u32[]{:S(2)}) copy-start(f32[1,4,512]{2,0,1:T(1,128)S(1)} %get-tuple-element.84) | copy-start | bytes 24580
  18.8 11.5 %copy-start.20 = (f32[1,4,512]{2,0,1:T(1,128)}, f32[1,4,512]{2,0,1:T(1,128)S(1)}, u32[]{:S(2)}) copy-start(f32[1,4,512]{2,0,1:T(1,128)S(1)} %get-tuple-element.85) | copy-start | bytes 24580
  18.8 11.5 %copy-start.22 = (f32[1,4,512]{2,0,1:T(1,128)}, f32[1,4,512]{2,0,1:T(1,128)S(1)}, u32[]{:S(2)}) copy-start(f32[1,4,512]{2,0,1:T(1,128)S(1)} %get-tuple-element.86) | copy-start | bytes 24580
  18.8 11.5 %copy-start.24 = (f32[1,4,512]{2,0,1:T(1,128)}, f32[1,4,512]{2,0,1:T(1,128)S(1)}, u32[]{:S(2)}) copy-start(f32[1,4,512]{2,0,1:T(1,128)S(1)} %get-tuple-element.87) | copy-start | bytes 24580
  18.8 11.5 %copy-start.26 = (f32[1,4,512]{2,0,1:T(1,128)}, f32[1,4,512]{2,0,1:T(1,128)S(1)}, u32[]{:S(2)}) copy-start(f32[1,4,512]{2,0,1:T(1,128)S(1)} %get-tuple-element.88) | copy-start | bytes 24580
  18.8 11.5 %copy-start.28 = (f32[1,4,512]{2,0,1:T(1,128)}, f32[1,4,512]{2,0,1:T(1,128)S(1)}, u32[]{:S(2)}) copy-start(f32[1,4,512]{2,0,1:T(1,128)S(1)} %get-tuple-element.89) | copy-start | bytes 24580
  18.8 11.5 %copy-start.30 = (f32[1,4,512]{2,0,1:T(1,128)}, f32[1,4,512]{2,0,1:T(1,128)S(1)}, u32[]{:S(2)}) copy-start(f32[1,4,512]{2,0,1:T(1,128)S(1)} %get-tuple-element.90) | copy-start | bytes 24580
  18.8 11.5 %copy-start.32 = (f32[1,4,512]{2,0,1:T(1,128)}, f32[1,4,512]{2,0,1:T(1,128)S(1)}, u32[]{:S(2)}) copy-start(f32[1,4,512]{2,0,1:T(1,128)S(1)} %get-tuple-element.91) | copy-start | bytes 24580
  18.8 11.5 %copy-start.34 = (f32[1,4,512]{2,0,1:T(1,128)}, f32[1,4,512]{2,0,1:T(1,128)S(1)}, u32[]{:S(2)}) copy-start(f32[1,4,512]{2,0,1:T(1,128)S(1)} %get-tuple-element.92) | copy-start | bytes 24580
  18.8 11.5 %copy-start.36 = (f32[1,4,512]{2,0,1:T(1,128)}, f32[1,4,512]{2,0,1:T(1,128)S(1)}, u32[]{:S(2)}) copy-start(f32[1,4,512]{2,0,1:T(1,128)S(1)} %get-tuple-element.93) | copy-start | bytes 24580
  18.9 11.5 %copy-start.38 = (f32[1,4,512]{2,0,1:T(1,128)}, f32[1,4,512]{2,0,1:T(1,128)S(1)}, u32[]{:S(2)}) copy-start(f32[1,4,512]{2,0,1:T(1,128)S(1)} %get-tuple-element.94) | copy-start | bytes 24580
  18.9 11.5 %copy-start.40 = (f32[1,4,512]{2,0,1:T(1,128)}, f32[1,4,512]{2,0,1:T(1,128)S(1)}, u32[]{:S(2)}) copy-start(f32[1,4,512]{2,0,1:T(1,128)S(1)} %get-tuple-element.95) | copy-start | bytes 24580
  18.9 11.5 %copy-start.42 = (f32[1,4,512]{2,0,1:T(1,128)}, f32[1,4,512]{2,0,1:T(1,128)S(1)}, u32[]{:S(2)}) copy-start(f32[1,4,512]{2,0,1:T(1,128)S(1)} %get-tuple-element.96) | copy-start | bytes 24580
  19.3 11.6 %copy-start.44 = (f32[2048]{0:T(1024)S(1)}, f32[2048]{0:T(1024)}, u32[]{:S(2)}) copy-start(f32[2048]{0:T(1024)} %param.10) | copy-start | bytes 24580
  30.4 2.4 %copy-start.14 = (bf16[256,4,4,64]{0,3,2,1:T(8,128)(2,1)S(1)}, bf16[256,4,4,64]{0,3,2,1:T(8,128)(2,1)}, u32[]{:S(2)}) copy-start(bf16[256,4,4,64]{0,3,2,1:T(8,128)(2,1)} %copy.19) | copy-start | bytes 1572868
  31.7 1.1 copy-start.11
  31.7 3.1 %copy-start = (bf16[256,2048]{1,0:T(8,128)(2,1)S(1)}, bf16[256,2048]{1,0:T(8,128)(2,1)}, u32[]{:S(2)}) copy-start(bf16[256,2048]{1,0:T(8,128)(2,1)} %param.11) | copy-start | bytes 3145732
  34.8 93.5 %copy-start.15 = (bf16[1,256,2048]{2,1,0:T(8,128)(2,1)S(1)}, bf16[1,256,2048]{2,1,0:T(8,128)(2,1)}, u32[]{:S(2)}) copy-start(bf16[1,256,2048]{2,1,0:T(8,128)(2,1)} %param.8) | copy-start | bytes 3145732
  128.3 6.2 %copy-start.2 = (bf16[8,256,256]{2,1,0:T(8,128)(2,1)}, bf16[8,256,256]{2,1,0:T(8,128)(2,1)S(1)}, u32[]{:S(2)}) copy-start(bf16[8,256,256]{2,1,0:T(8,128)(2,1)S(1)} %get-tuple-element.24) | copy-start | bytes 3145732
  141.7 4.4 %copy-start.6 = (bf16[256,2048]{1,0:T(8,128)(2,1)}, bf16[256,2048]{1,0:T(8,128)(2,1)S(1)}, u32[]{:S(2)}) copy-start(bf16[256,2048]{1,0:T(8,128)(2,1)S(1)} %get-tuple-element.71) | copy-start | bytes 3145732
  141.7 8.9 %copy-start.3 = (bf16[8,256,256]{2,1,0:T(8,128)(2,1)S(1)}, bf16[8,256,256]{2,1,0:T(8,128)(2,1)}, u32[]{:S(2)}) copy-start(bf16[8,256,256]{2,1,0:T(8,128)(2,1)} %copy-done.2) | copy-start | bytes 3145732
  150.7 3.6 %copy-start.12 = (bf16[256,2048]{1,0:T(8,128)(2,1)S(1)}, bf16[256,2048]{1,0:T(8,128)(2,1)}, u32[]{:S(2)}) copy-start(bf16[256,2048]{1,0:T(8,128)(2,1)} %copy-done.11) | copy-start | bytes 3145732
  150.7 3.6 %copy-start.13 = (bf16[256,4,4,64]{0,3,2,1:T(8,128)(2,1)S(1)}, bf16[256,4,4,64]{0,3,2,1:T(8,128)(2,1)}, u32[]{:S(2)}) copy-start(bf16[256,4,4,64]{0,3,2,1:T(8,128)(2,1)} %copy.21) | copy-start | bytes 1572868
  206.9 15.5 %copy-start.7 = (bf16[256,2048]{1,0:T(8,128)(2,1)S(1)}, bf16[256,2048]{1,0:T(8,128)(2,1)}, u32[]{:S(2)}) copy-start(bf16[256,2048]{1,0:T(8,128)(2,1)} %copy-done.6) | copy-start | bytes 3145732
  222.4 1.2 copy-start.5
  222.4 1.5 copy-start.9
  222.4 1.5 copy-start.17
  222.4 1.5 copy-start.19
  222.4 1.5 copy-start.21
  222.5 1.5 copy-start.23
  222.5 1.5 copy-start.25
  222.5 1.5 copy-start.27
  222.5 1.5 copy-start.29
  222.5 1.5 copy-start.31
  222.5 1.5 copy-start.33
  222.5 1.5 copy-start.35
  222.5 1.5 copy-start.37
  222.5 1.5 copy-start.39
  222.5 1.5 copy-start.41
  222.6 1.5 copy-start.43

commit v5 on v4

--- a/solution.py
+++ b/solution.py
@@ -262,7 +262,7 @@
     sig = jax.nn.sigmoid(scaled)
     activated = (scaled * sig).astype(jnp.bfloat16)
 
-    half = channels // 2
+    low = channels // 4
     nz, piece = ndp // 2, rows // nsp
     core = lax.rem(lax.axis_index("dp"), 2)
     by_core = up.reshape(length, nz, 2, nsp, piece)
@@ -271,24 +271,24 @@
         columns = lax.dynamic_index_in_dim(by_core, which, 2, keepdims=False)
         columns = jnp.swapaxes(columns, 1, 2).reshape(length, nsp * nz * piece)
         return lax.dot_general(
-            columns, activated[:, half:], (((0,), (0,)), ((), ())), preferred_element_type=f32
+            columns, activated[:, low:], (((0,), (0,)), ((), ())), preferred_element_type=f32
         )
 
     weight, act_all, up_columns, from_partner = exchange(
         2,
         ("spread", "dp", out_weight.reshape(nsp, rows // nsp, channels)),
-        ("line", "dp", activated[:, :half]),
+        ("line", "dp", activated[:, :low]),
         ("later", "dp", up_blocks),
         ("pair", "dp", partial(1 - core).astype(jnp.bfloat16)),
     )
     weight = weight.reshape(ndp * rows, channels)
-    act_all = act_all.reshape(ndp * length, half)
+    act_all = act_all.reshape(ndp * length, low)
     up_columns = up_columns.reshape(ndp * length, rows)
     owned = lax.dot_general(
         up_columns, act_all, (((0,), (0,)), ((), ())), preferred_element_type=f32
     )
     summed = (partial(core) + from_partner.astype(f32)).astype(jnp.bfloat16)
-    summed = summed.reshape(nsp, nz, piece, half)
+    summed = summed.reshape(nsp, nz, piece, channels - low)
 
     grad_act = jnp.dot(up, weight, preferred_element_type=f32)
     grad_scaled = grad_act * sig * (1.0 + scaled * (1.0 - sig))
@@ -304,7 +304,7 @@
         3,
         ("prev", "sp", grad_conv[:edge]),
         ("gather", "sp", gain_part[None]),
-        ("scatter", "sp", owned.astype(jnp.bfloat16).reshape(nsp, piece, half)),
+        ("scatter", "sp", owned.astype(jnp.bfloat16).reshape(nsp, piece, low)),
         ("scatter", "sp", summed),
     )
     after = jnp.where(at_end, 0, after)[:halo]
@@ -337,7 +337,7 @@
     grad_gain = jnp.sum(gain_got, axis=0)[0]
     grad_taps = jnp.sum(tap_got, axis=0)
     grad_weight = jnp.concatenate(
-        [low_weight.reshape(rows, half), high_weight.reshape(rows, half)], axis=1
+        [low_weight.reshape(rows, low), high_weight.reshape(rows, channels - low)], axis=1
     ).astype(f32)
     return (grad_value[None], grad_gate[None], grad_taps, grad_gain, grad_weight)
 

time: 237 us -> 237 us (level)
    another operation x1, local copies, waits for them, and re-layouts: 3.63 us -> 0.43 us  [body(): jnp.stack(terms).reshape(tap_count, nsp, width)]
    dot_general x2, matrix products: 2.75 us -> 5.43 us  [partial(): lax.dot_general(columns, activated[:, low:], (((0,), (0,)), ((), ())), pr...]
    unnamed x91 -> x129, local copies, waits for them, and re-layouts: 5.14 us -> 6.07 us
where the time goes in v5:
time: 237 us
  Pallas kernels  168 us (71%)
  other arithmetic  41.6 us (18%)
  matrix products  13.7 us (6%)
  local copies, waits for them, and re-layouts  11 us (5%)
    pallas_call x5, Pallas kernels, exchange(): pl.pallas_call(functools.partial(run, axes, tuple(((kind, axis) for kind,...  168 us
    reduce_sum x1, other arithmetic, body(): mean = jnp.mean(conv, axis=-1, keepdims=True)  11 us
    reduce_sum x2, other arithmetic, body(): terms.append(jnp.sum(here * padded[j:j + length], axis=0))  10.3 us
    broadcast_in_dim x1, other arithmetic, body(): grad_gate[None]  9.49 us
    dot_general x1, matrix products, body(): grad_act = jnp.dot(up, weight, preferred_element_type=f32)  6.21 us
    unnamed x129, local copies, waits for them, and re-layouts  6.07 us
    dot_general x2, matrix products, partial(): lax.dot_general(columns, activated[:, low:], (((0,), (0,)), ((), ())), pr...  5.43 us

profile of v5, /device:TPU:0, one launch (start us, length us, event | category | flops | bytes accessed | tf_op | source)
XLA Modules:
  0.0 236.6 jit_solution(8628433393528213056)
XLA Ops:
  0.6 1.5 copy.16
  2.1 0.0 copy-start.11
  2.1 0.1 dynamic-slice_bitcast_fusion
  2.3 0.9 copy.21
  3.1 0.8 copy.19
  4.0 1.5 copy.17
  5.5 0.6 fusion.88
  6.0 0.2 convert_element_type.73
  6.3 0.0 copy-start.3
  6.3 0.2 convert_element_type.74
  6.5 0.1 fusion.100.refs_0_
  6.6 0.5 copy-done.3
  7.1 10.6 %shard_map.101 = (bf16[32,2048]{1,0:T(8,128)(2,1)S(1)}, f32[4,31,512]{2,1,0:T(8,128)S(1)}) custom-call(bf16[32,2048]{1,0:T(8,128)(2,1)S(1)} %fusion.100.refs_0_, f32[31,512]{1,0:T(8,128)S(1)} %copy-done.3), custom_call_target="tpu_custom_call" | custom-call | tf_op jit(solution)/shard_map/pallas_call | solution.py:213
  17.8 0.1 fusion.104
  17.9 0.1 fusion.103
  18.2 0.3 maximum_convert_fusion
  18.6 11.0 %convert_reduce_fusion = (f32[256]{0:T(256)S(1)}, bf16[256,2048]{1,0:T(8,128)(2,1)S(1)}) fusion(f32[286,2048]{1,0:T(8,128)S(1)} %maximum_convert_fusion, f32[2048]{0:T(1024)S(1)} %bitcast.170, f32[2048]{0:T(1024)S(1)} %bitcast.172, f32[2048]{0:T(1024)S(1)} %bitcast.174, f32[2048]{0:T(1024)S(1)} %bitcast.176, f32[2048]{0:T(1024)S(1)} %bitcast.178, ...), kind=kLoop, calls=%fused_computation.39 | loop fusion | flops 33554176 | bytes 66315264 | tf_op jit(solution)/shard_map/reduce_sum | solution.py:257
  29.7 0.0 copy-start.14
  29.8 0.4 fusion.21
  30.2 0.9 fusion.14
  31.1 0.9 copy-done.12
  32.1 2.7 %convolution_convert_fusion.refs_3_ = bf16[1024,1536]{1,0:T(8,128)(2,1)} fusion(bf16[256,1024]{0,1:T(8,128)(2,1)S(1)} %bitcast.142, bf16[256,2048]{1,0:T(8,128)(2,1)S(1)} %fusion.14), kind=kOutput, calls=%fused_computation.32 | convolution fusion | flops 806879232 | bytes 4456448 | tf_op jit(solution)/shard_map/dot_general | solution.py:273
  34.8 76.3 %shard_map.102 = (bf16[8,4,64,2048]{3,2,1,0:T(8,128)(2,1)}, bf16[8,256,512]{2,1,0:T(8,128)(2,1)S(1)}, bf16[8,256,256]{2,1,0:T(8,128)(2,1)S(1)}, bf16[1024,1536]{1,0:T(8,128)(2,1)}) custom-call(bf16[4,64,2048]{2,1,0:T(8,128)(2,1)S(1)} %bitcast.131, bf16[256,512]{1,0:T(8,128)(2,1)S(1)} %slice.564.refs_1_, bf16[8,256,256]{2,1,0:T(8,128)(2,1)S(1)} %bitcast.129, ...), custom_call_target="tpu_custom_call" | custom-call | tf_op jit(solution)/shard_map/pallas_call | solution.py:213
  111.2 6.2 %fusion.20 = (f32[2048]{0:T(1024)S(1)}, f32[256]{0:T(256)S(1)}, f32[256]{0:T(256)S(1)}, f32[256,2048]{1,0:T(8,128)S(1)}) fusion(bf16[256,2048]{1,0:T(8,128)(2,1)S(1)} %get-tuple-element.75, f32[256]{0:T(256)S(1)} %add_rsqrt_fusion, f32[256]{0:T(256)S(1)} %broadcast_multiply_fusion.2, f32[2048]{0:T(1024)S(1)} %copy-done.63, ...), kind=kOutput, calls=%fused_computation.58 | convolution fusion | flops 2156918272 | bytes 12603392 | tf_op jit(solution)/shard_map/dot_general | solution.py:293
  117.4 6.6 %fusion.56 = (f32[2048]{0:T(1024)S(1)}, f32[2048]{0:T(1024)S(1)}, f32[2048]{0:T(1024)S(1)}, f32[2048]{0:T(1024)S(1)}, f32[2048]{0:T(1024)S(1)}, /*index=5*/f32[2...) fusion(f32[286,2048]{1,0:T(8,128)S(1)} %maximum_convert_fusion,, ...), kind=kLoop, calls=%fused_computation.94 | loop fusion | flops 24080384 | bytes 42102784 | tf_op jit(solution)/shard_map/reduce_sum | solution.py:318
  124.0 0.0 copy-start.7
  124.0 3.7 %fusion.55 = (f32[2048]{0:T(1024)S(1)}, f32[2048]{0:T(1024)S(1)}, f32[2048]{0:T(1024)S(1)}, f32[2048]{0:T(1024)S(1)}, f32[2048]{0:T(1024)S(1)}, /*index=5*/f32[2...) fusion(bf16[256,2048]{1,0:T(8,128)(2,1)S(1)} %get-tuple-element, ...), kind=kLoop, calls=%fused_computation.93 | loop fusion | flops 14129152 | bytes 28418048 | tf_op jit(solution)/shard_map/reduce_sum | solution.py:318
  127.8 0.4 stack.127
  128.2 1.1 slice.566.refs_0_
  129.3 2.0 fusion.89
  131.4 2.7 %add_convert_fusion = bf16[1024,1536]{1,0:T(8,128)(2,1)} fusion(bf16[1024,1536]{1,0:T(8,128)(2,1)S(1)} %copy-done.15, bf16[256,1024]{0,1:T(8,128)(2,1)S(1)} %bitcast.143, bf16[256,2048]{1,0:T(8,128)(2,1)S(1)} %copy-done.13), kind=kOutput, calls=%fused_computation.31 | convolution fusion | flops 810024960 | bytes 7602176 | tf_op jit(solution)/shard_map/dot_general | solution.py:273
  134.1 46.0 %shard_map.103 = (bf16[32,2048]{1,0:T(8,128)(2,1)S(1)}, f32[4,1,2048]{2,1,0:T(1,128)S(1)}, bf16[4,64,512]{2,1,0:T(8,128)(2,1)S(1)}, bf16[4,4,64,1536]{3,2,1,0:T(8,128)(2,1)S(1)}) custom-call(bf16[32,2048]{1,0:T(8,128)(2,1)S(1)} %slice.566.refs_0_, f32[1,2048]{1,0:T(1,128)S(1)} %bitcast.138, bf16[4,64,512]{2,1,0:T(8,128)(2,1)S(1)} %bitcast.134, ...), custom_call_target="tpu_custom_call" | custom-call | tf_op jit(solution)/shard_map/pallas_call | solution.py:213
  180.1 0.7 copy-done.2
  180.8 0.6 slice_select_fusion
  181.5 1.0 reduce_sum.436.refs_2_
  182.5 1.6 reduce_sum.437.refs_3_
  184.0 1.1 copy-done
  185.2 18.8 %shard_map.104 = (f32[8,1,2048]{2,1,0:T(1,128)S(1)}, f32[4,31,512]{2,1,0:T(8,128)S(1)}, bf16[4,64,512]{2,1,0:T(8,128)(2,1)S(1)}, bf16[4,64,1536]{2,1,0:T(8,128)(2,1)S(1)}) custom-call(f32[1,2048]{1,0:T(1,128)S(1)} %bitcast.137, f32[4,31,512]{2,1,0:T(8,128)S(1)} %bitcast.130, bf16[64,512]{1,0:T(8,128)(2,1)S(1)} %reduce_sum.436.refs_2_, ...), custom_call_target="tpu_custom_call" | custom-call | tf_op jit(solution)/shard_map/pallas_call | solution.py:213
  204.0 0.7 reduce_sum.441
  204.7 0.1 reduce_sum.439.refs_1_
  204.8 16.7 %shard_map.105 = (f32[8,31,512]{2,1,0:T(8,128)S(1)}, bf16[4,64,1536]{2,1,0:T(8,128)(2,1)S(1)}) custom-call(f32[31,512]{1,0:T(8,128)S(1)} %reduce_sum.438.refs_0_, bf16[64,1536]{1,0:T(8,128)(2,1)S(1)} %reduce_sum.439.refs_1_), custom_call_target="tpu_custom_call" | custom-call | tf_op jit(solution)/shard_map/pallas_call | solution.py:213
  221.5 0.7 reduce_sum.440
  222.2 1.6 maximum_convert_fusion.2
  224.0 0.3 maximum_convert_fusion.1
  224.3 0.7 copy-done.6
  225.0 0.3 copy-done.10
  225.5 9.5 %fusion.90 = (bf16[1,256,2048]{2,1,0:T(8,128)(2,1)}, bf16[256,2048]{1,0:T(8,128)(2,1)S(1)}) fusion(bf16[1,256,2048]{2,1,0:T(8,128)(2,1)S(1)} %copy-done.10, bf16[1,256,2048]{2,1,0:T(8,128)(2,1)S(1)} %copy-done.6, f32[286,2048]{1,0:T(8,128)S(1)} %maximum_convert_fusion.1, f32[2048]{0:T(1024)S(1)} %bitcast.171, f32[2048]{0:T(1024)S(1)} %bitcast.173, ...), kind=kLoop, calls=%fused_computation.167 | loop fusion | flops 38273024 | bytes 69459968 | tf_op jit(solution)/shard_map/broadcast_in_dim | solution.py:342
  235.0 1.6 fusion.91
  (125 shorter events, 0.4 us)
Async XLA Ops:
  2.1 1.8 copy-start.11
  2.3 3.2 %copy-start.5 = (bf16[1,256,2048]{2,1,0:T(8,128)(2,1)S(1)}, bf16[1,256,2048]{2,1,0:T(8,128)(2,1)}, u32[]{:S(2)}) copy-start(bf16[1,256,2048]{2,1,0:T(8,128)(2,1)} %param.7) | copy-start | bytes 3145732
  2.3 3.2 %copy-start.9 = (bf16[1,256,2048]{2,1,0:T(8,128)(2,1)S(1)}, bf16[1,256,2048]{2,1,0:T(8,128)(2,1)}, u32[]{:S(2)}) copy-start(bf16[1,256,2048]{2,1,0:T(8,128)(2,1)} %param.6) | copy-start | bytes 3145732
  18.0 11.6 %copy-start.25 = (f32[1,4,512]{2,0,1:T(1,128)}, f32[1,4,512]{2,0,1:T(1,128)S(1)}, u32[]{:S(2)}) copy-start(f32[1,4,512]{2,0,1:T(1,128)S(1)} %get-tuple-element.78) | copy-start | bytes 24580
  18.0 11.6 %copy-start.27 = (f32[1,4,512]{2,0,1:T(1,128)}, f32[1,4,512]{2,0,1:T(1,128)S(1)}, u32[]{:S(2)}) copy-start(f32[1,4,512]{2,0,1:T(1,128)S(1)} %get-tuple-element.79) | copy-start | bytes 24580
  18.0 11.6 %copy-start.29 = (f32[1,4,512]{2,0,1:T(1,128)}, f32[1,4,512]{2,0,1:T(1,128)S(1)}, u32[]{:S(2)}) copy-start(f32[1,4,512]{2,0,1:T(1,128)S(1)} %get-tuple-element.80) | copy-start | bytes 24580
  18.0 11.6 %copy-start.31 = (f32[1,4,512]{2,0,1:T(1,128)}, f32[1,4,512]{2,0,1:T(1,128)S(1)}, u32[]{:S(2)}) copy-start(f32[1,4,512]{2,0,1:T(1,128)S(1)} %get-tuple-element.81) | copy-start | bytes 24580
  18.0 11.6 %copy-start.33 = (f32[1,4,512]{2,0,1:T(1,128)}, f32[1,4,512]{2,0,1:T(1,128)S(1)}, u32[]{:S(2)}) copy-start(f32[1,4,512]{2,0,1:T(1,128)S(1)} %get-tuple-element.82) | copy-start | bytes 24580
  18.0 11.6 %copy-start.35 = (f32[1,4,512]{2,0,1:T(1,128)}, f32[1,4,512]{2,0,1:T(1,128)S(1)}, u32[]{:S(2)}) copy-start(f32[1,4,512]{2,0,1:T(1,128)S(1)} %get-tuple-element.83) | copy-start | bytes 24580
  18.0 11.6 %copy-start.37 = (f32[1,4,512]{2,0,1:T(1,128)}, f32[1,4,512]{2,0,1:T(1,128)S(1)}, u32[]{:S(2)}) copy-start(f32[1,4,512]{2,0,1:T(1,128)S(1)} %get-tuple-element.84) | copy-start | bytes 24580
  18.1 11.6 %copy-start.39 = (f32[1,4,512]{2,0,1:T(1,128)}, f32[1,4,512]{2,0,1:T(1,128)S(1)}, u32[]{:S(2)}) copy-start(f32[1,4,512]{2,0,1:T(1,128)S(1)} %get-tuple-element.85) | copy-start | bytes 24580
  18.1 11.6 %copy-start.41 = (f32[1,4,512]{2,0,1:T(1,128)}, f32[1,4,512]{2,0,1:T(1,128)S(1)}, u32[]{:S(2)}) copy-start(f32[1,4,512]{2,0,1:T(1,128)S(1)} %get-tuple-element.86) | copy-start | bytes 24580
  18.1 11.6 %copy-start.43 = (f32[1,4,512]{2,0,1:T(1,128)}, f32[1,4,512]{2,0,1:T(1,128)S(1)}, u32[]{:S(2)}) copy-start(f32[1,4,512]{2,0,1:T(1,128)S(1)} %get-tuple-element.87) | copy-start | bytes 24580
  18.1 11.6 %copy-start.45 = (f32[1,4,512]{2,0,1:T(1,128)}, f32[1,4,512]{2,0,1:T(1,128)S(1)}, u32[]{:S(2)}) copy-start(f32[1,4,512]{2,0,1:T(1,128)S(1)} %get-tuple-element.88) | copy-start | bytes 24580
  18.1 11.6 %copy-start.47 = (f32[1,4,512]{2,0,1:T(1,128)}, f32[1,4,512]{2,0,1:T(1,128)S(1)}, u32[]{:S(2)}) copy-start(f32[1,4,512]{2,0,1:T(1,128)S(1)} %get-tuple-element.89) | copy-start | bytes 24580
  18.1 11.6 %copy-start.49 = (f32[1,4,512]{2,0,1:T(1,128)}, f32[1,4,512]{2,0,1:T(1,128)S(1)}, u32[]{:S(2)}) copy-start(f32[1,4,512]{2,0,1:T(1,128)S(1)} %get-tuple-element.90) | copy-start | bytes 24580
  18.1 11.6 %copy-start.51 = (f32[1,4,512]{2,0,1:T(1,128)}, f32[1,4,512]{2,0,1:T(1,128)S(1)}, u32[]{:S(2)}) copy-start(f32[1,4,512]{2,0,1:T(1,128)S(1)} %get-tuple-element.91) | copy-start | bytes 24580
  18.1 11.6 %copy-start.53 = (f32[1,4,512]{2,0,1:T(1,128)}, f32[1,4,512]{2,0,1:T(1,128)S(1)}, u32[]{:S(2)}) copy-start(f32[1,4,512]{2,0,1:T(1,128)S(1)} %get-tuple-element.92) | copy-start | bytes 24580
  18.1 11.6 %copy-start.55 = (f32[1,4,512]{2,0,1:T(1,128)}, f32[1,4,512]{2,0,1:T(1,128)S(1)}, u32[]{:S(2)}) copy-start(f32[1,4,512]{2,0,1:T(1,128)S(1)} %get-tuple-element.93) | copy-start | bytes 24580
  18.1 11.6 %copy-start.57 = (f32[1,4,512]{2,0,1:T(1,128)}, f32[1,4,512]{2,0,1:T(1,128)S(1)}, u32[]{:S(2)}) copy-start(f32[1,4,512]{2,0,1:T(1,128)S(1)} %get-tuple-element.94) | copy-start | bytes 24580
  18.2 11.6 %copy-start.59 = (f32[1,4,512]{2,0,1:T(1,128)}, f32[1,4,512]{2,0,1:T(1,128)S(1)}, u32[]{:S(2)}) copy-start(f32[1,4,512]{2,0,1:T(1,128)S(1)} %get-tuple-element.95) | copy-start | bytes 24580
  18.2 11.6 %copy-start.61 = (f32[1,4,512]{2,0,1:T(1,128)}, f32[1,4,512]{2,0,1:T(1,128)S(1)}, u32[]{:S(2)}) copy-start(f32[1,4,512]{2,0,1:T(1,128)S(1)} %get-tuple-element.96) | copy-start | bytes 24580
  18.6 11.6 %copy-start.63 = (f32[2048]{0:T(1024)S(1)}, f32[2048]{0:T(1024)}, u32[]{:S(2)}) copy-start(f32[2048]{0:T(1024)} %param.10) | copy-start | bytes 24580
  29.7 2.3 copy-start.14
  32.1 2.7 %copy-start.1 = (bf16[256,2048]{1,0:T(8,128)(2,1)S(1)}, bf16[256,2048]{1,0:T(8,128)(2,1)}, u32[]{:S(2)}) copy-start(bf16[256,2048]{1,0:T(8,128)(2,1)} %param.11) | copy-start | bytes 3145732
  34.8 76.3 %copy-start.17 = (bf16[1,256,2048]{2,1,0:T(8,128)(2,1)S(1)}, bf16[1,256,2048]{2,1,0:T(8,128)(2,1)}, u32[]{:S(2)}) copy-start(bf16[1,256,2048]{2,1,0:T(8,128)(2,1)} %param.8) | copy-start | bytes 3145732
  111.1 6.2 %copy-start.4 = (bf16[8,256,256]{2,1,0:T(8,128)(2,1)}, bf16[8,256,256]{2,1,0:T(8,128)(2,1)S(1)}, u32[]{:S(2)}) copy-start(bf16[8,256,256]{2,1,0:T(8,128)(2,1)S(1)} %get-tuple-element.24) | copy-start | bytes 3145732
  124.0 3.8 %copy-start.7 = (bf16[256,2048]{1,0:T(8,128)(2,1)}, bf16[256,2048]{1,0:T(8,128)(2,1)S(1)}, u32[]{:S(2)}) copy-start(bf16[256,2048]{1,0:T(8,128)(2,1)S(1)} %get-tuple-element.71) | copy-start | bytes 3145732
  124.0 7.3 %copy-start.16 = (bf16[256,4,4,64]{0,3,2,1:T(8,128)(2,1)S(1)}, bf16[256,4,4,64]{0,3,2,1:T(8,128)(2,1)}, u32[]{:S(2)}) copy-start(bf16[256,4,4,64]{0,3,2,1:T(8,128)(2,1)} %copy.21) | copy-start | bytes 1572868
  128.2 3.1 %copy-start.15 = (bf16[1024,1536]{1,0:T(8,128)(2,1)S(1)}, bf16[1024,1536]{1,0:T(8,128)(2,1)}, u32[]{:S(2)}) copy-start(bf16[1024,1536]{1,0:T(8,128)(2,1)} %get-tuple-element.26) | copy-start | bytes 9437188
  129.3 2.1 copy-start.13
  204.8 18.9 %copy-start.8 = (bf16[256,2048]{1,0:T(8,128)(2,1)S(1)}, bf16[256,2048]{1,0:T(8,128)(2,1)}, u32[]{:S(2)}) copy-start(bf16[256,2048]{1,0:T(8,128)(2,1)} %copy-done.7) | copy-start | bytes 3145732
  204.8 18.9 %copy-start.18 = (bf16[30,2048]{1,0:T(8,128)(2,1)S(1)}, bf16[30,2048]{1,0:T(8,128)(2,1)}, u32[]{:S(2)}) copy-start(bf16[30,2048]{1,0:T(8,128)(2,1)} %slice_select_fusion) | copy-start | bytes 368644
  223.8 1.5 copy-start.10
  223.8 1.5 copy-start.20
  223.8 1.5 copy-start.22
  223.8 1.5 copy-start.24
  223.8 1.5 copy-start.26
  223.8 1.5 copy-start.28
  223.8 1.5 copy-start.30
  223.8 1.5 copy-start.32
  223.9 1.5 copy-start.34
  223.9 1.5 copy-start.36
  223.9 1.5 copy-start.38
  223.9 1.5 copy-start.40
  223.9 1.5 copy-start.42
  223.9 1.5 copy-start.44
  223.9 1.5 copy-start.46
  (16 other events, 19.1 us)

commit v6 on v5

--- a/solution.py
+++ b/solution.py
@@ -262,7 +262,7 @@
     sig = jax.nn.sigmoid(scaled)
     activated = (scaled * sig).astype(jnp.bfloat16)
 
-    low = channels // 4
+    low = channels * 3 // 8
     nz, piece = ndp // 2, rows // nsp
     core = lax.rem(lax.axis_index("dp"), 2)
     by_core = up.reshape(length, nz, 2, nsp, piece)

time: 237 us -> 239 us (level)
  matrix products: 13.7 us -> 16.8 us
    dot_general x1, matrix products: 6.21 us -> 8.87 us  [body(): grad_act = jnp.dot(up, weight, preferred_element_type=f32)]
    unnamed x129 -> x159, local copies, waits for them, and re-layouts: 6.07 us -> 5.09 us
where the time goes in v6:
time: 239 us; the launch traced here: 238 us
  Pallas kernels  168 us (70%)
  other arithmetic  41.7 us (17%)
  matrix products  16.8 us (7%)
  local copies, waits for them, and re-layouts  9 us (4%)
    pallas_call x5, Pallas kernels, exchange(): pl.pallas_call(functools.partial(run, axes, tuple(((kind, axis) for kind,...  168 us
    reduce_sum x2, other arithmetic, body(): terms.append(jnp.sum(here * padded[j:j + length], axis=0))  11.5 us
    reduce_sum x1, other arithmetic, body(): mean = jnp.mean(conv, axis=-1, keepdims=True)  11 us
    broadcast_in_dim x1, other arithmetic, body(): grad_gate[None]  9.49 us
    dot_general x1, matrix products, body(): grad_act = jnp.dot(up, weight, preferred_element_type=f32)  8.87 us
    unnamed x159, local copies, waits for them, and re-layouts  5.09 us
    dot_general x2, matrix products, partial(): lax.dot_general(columns, activated[:, low:], (((0,), (0,)), ((), ())), pr...  4.85 us

profile of v6, /device:TPU:0, one launch (start us, length us, event | category | flops | bytes accessed | tf_op | source)
XLA Modules:
  0.0 237.7 jit_solution(7423676626106836246)
XLA Ops:
  0.6 1.5 copy.16
  2.1 0.0 copy-start.11
  2.1 0.1 dynamic-slice_bitcast_fusion
  2.3 0.0 copy-start.5
  2.3 0.8 copy.21
  3.1 0.8 copy.19
  3.9 1.5 copy.17
  5.5 0.6 fusion.88
  6.0 0.2 convert_element_type.73
  6.3 0.2 convert_element_type.74
  6.5 0.1 fusion.100.refs_0_
  6.6 0.5 copy-done.4
  7.1 10.6 %shard_map.101 = (bf16[32,2048]{1,0:T(8,128)(2,1)S(1)}, f32[4,31,512]{2,1,0:T(8,128)S(1)}) custom-call(bf16[32,2048]{1,0:T(8,128)(2,1)S(1)} %fusion.100.refs_0_, f32[31,512]{1,0:T(8,128)S(1)} %copy-done.4), custom_call_target="tpu_custom_call" | custom-call | tf_op jit(solution)/shard_map/pallas_call | solution.py:213
  17.7 0.1 fusion.104
  17.9 0.1 fusion.103
  18.3 0.3 maximum_convert_fusion
  18.7 0.0 copy-start.78
  18.7 11.0 %convert_reduce_fusion = (f32[256]{0:T(256)S(1)}, bf16[256,2048]{1,0:T(8,128)(2,1)S(1)}) fusion(f32[286,2048]{1,0:T(8,128)S(1)} %maximum_convert_fusion, f32[2048]{0:T(1024)S(1)} %bitcast.170, f32[2048]{0:T(1024)S(1)} %bitcast.172, f32[2048]{0:T(1024)S(1)} %bitcast.174, f32[2048]{0:T(1024)S(1)} %bitcast.176, f32[2048]{0:T(1024)S(1)} %bitcast.178, ...), kind=kLoop, calls=%fused_computation.39 | loop fusion | flops 33554176 | bytes 66315264 | tf_op jit(solution)/shard_map/reduce_sum | solution.py:257
  29.9 0.0 copy-start.15
  29.9 0.4 fusion.21
  30.3 0.9 fusion.14
  31.2 0.0 copy-start.12
  31.3 0.9 copy-done.12
  32.2 2.4 %convolution_convert_fusion.refs_3_ = bf16[1024,1280]{1,0:T(8,128)(2,1)} fusion(bf16[256,1024]{0,1:T(8,128)(2,1)S(1)} %bitcast.143, bf16[256,2048]{1,0:T(8,128)(2,1)S(1)} %fusion.14), kind=kOutput, calls=%fused_computation.32 | convolution fusion | flops 672399360 | bytes 3801088 | tf_op jit(solution)/shard_map/dot_general | solution.py:273
  34.6 84.8 %shard_map.102 = (bf16[8,4,64,2048]{3,2,1,0:T(8,128)(2,1)}, bf16[8,256,768]{2,1,0:T(8,128)(2,1)}, bf16[8,256,256]{2,1,0:T(8,128)(2,1)S(1)}, bf16[1024,1280]{1,0:T(8,128)(2,1)S(1)}) custom-call(bf16[4,64,2048]{2,1,0:T(8,128)(2,1)S(1)} %bitcast.130, bf16[256,768]{1,0:T(8,128)(2,1)S(1)} %slice.564.refs_1_, bf16[8,256,256]{2,1,0:T(8,128)(2,1)S(1)} %bitcast.129, ...), custom_call_target="tpu_custom_call" | custom-call | tf_op jit(solution)/shard_map/pallas_call | solution.py:213
  119.4 8.9 %fusion.20 = (f32[2048]{0:T(1024)S(1)}, f32[256]{0:T(256)S(1)}, f32[256]{0:T(256)S(1)}, f32[256,2048]{1,0:T(8,128)}) fusion(bf16[256,2048]{1,0:T(8,128)(2,1)S(1)} %get-tuple-element.75, f32[256]{0:T(256)S(1)} %add_rsqrt_fusion, f32[256]{0:T(256)S(1)} %broadcast_multiply_fusion.2, f32[2048]{0:T(1024)S(1)} %copy-done.78, bf16[2048,2048]{1,0:T(8,128)(2,1)} %bitcast.237, ...), kind=kOutput, calls=%fused_computation.58 | convolution fusion | flops 2156918272 | bytes 12603392 | tf_op jit(solution)/shard_map/dot_general | solution.py:293
  128.3 7.9 %fusion.56 = (f32[2048]{0:T(1024)S(1)}, f32[2048]{0:T(1024)S(1)}, f32[2048]{0:T(1024)S(1)}, f32[2048]{0:T(1024)S(1)}, f32[2048]{0:T(1024)S(1)}, /*index=5*/f32[2...) fusion(f32[286,2048]{1,0:T(8,128)S(1)} %maximum_convert_fusion,, ...), kind=kLoop, calls=%fused_computation.94 | loop fusion | flops 24080384 | bytes 42102784 | tf_op jit(solution)/shard_map/reduce_sum | solution.py:318
  136.2 0.0 copy-start.7
  136.2 3.6 %fusion.55 = (f32[2048]{0:T(1024)S(1)}, f32[2048]{0:T(1024)S(1)}, f32[2048]{0:T(1024)S(1)}, f32[2048]{0:T(1024)S(1)}, f32[2048]{0:T(1024)S(1)}, /*index=5*/f32[2...) fusion(bf16[256,2048]{1,0:T(8,128)(2,1)S(1)} %get-tuple-element, ...), kind=kLoop, calls=%fused_computation.93 | loop fusion | flops 14129152 | bytes 28418048 | tf_op jit(solution)/shard_map/reduce_sum | solution.py:318
  139.8 0.4 stack.127
  140.3 3.1 %fusion.89 = bf16[256,768]{1,0:T(8,128)(2,1)S(1)} fusion(bf16[8,256,256]{2,1,0:T(8,128)(2,1)S(1)} %get-tuple-element.24, bf16[8,256,768]{2,1,0:T(8,128)(2,1)} %get-tuple-element.25), kind=kOutput, calls=%fused_computation.164 | convolution fusion | flops 805502976 | bytes 4587520 | tf_op jit(solution)/shard_map/dot_general | solution.py:287
  143.4 2.4 %add_convert_fusion = bf16[1024,1280]{1,0:T(8,128)(2,1)} fusion(bf16[1024,1280]{1,0:T(8,128)(2,1)S(1)} %copy-done.1, bf16[256,1024]{0,1:T(8,128)(2,1)S(1)} %bitcast.142, bf16[256,2048]{1,0:T(8,128)(2,1)S(1)} %copy-done.13), kind=kOutput, calls=%fused_computation.31 | convolution fusion | flops 675020800 | bytes 6422528 | tf_op jit(solution)/shard_map/dot_general | solution.py:273
  145.8 41.7 %shard_map.103 = (bf16[32,2048]{1,0:T(8,128)(2,1)S(1)}, f32[4,1,2048]{2,1,0:T(1,128)S(1)}, bf16[4,64,768]{2,1,0:T(8,128)(2,1)S(1)}, bf16[4,4,64,1280]{3,2,1,0:T(8,128)(2,1)S(1)}) custom-call(bf16[32,2048]{1,0:T(8,128)(2,1)S(1)} %slice.566.refs_0_, f32[1,2048]{1,0:T(1,128)S(1)} %bitcast.138, bf16[4,64,768]{2,1,0:T(8,128)(2,1)S(1)} %bitcast.134, ...), custom_call_target="tpu_custom_call" | custom-call | tf_op jit(solution)/shard_map/pallas_call | solution.py:213
  187.5 0.7 slice_select_fusion
  188.2 0.7 reduce_sum.436.refs_2_
  188.9 0.7 reduce_sum.437.refs_3_
  189.7 0.9 copy-done.3
  190.6 16.7 %shard_map.104 = (f32[8,1,2048]{2,1,0:T(1,128)S(1)}, f32[4,31,512]{2,1,0:T(8,128)S(1)}, bf16[4,64,768]{2,1,0:T(8,128)(2,1)S(1)}, bf16[4,64,1280]{2,1,0:T(8,128)(2,1)S(1)}) custom-call(f32[1,2048]{1,0:T(1,128)S(1)} %bitcast.137, f32[4,31,512]{2,1,0:T(8,128)S(1)} %bitcast.131, bf16[64,768]{1,0:T(8,128)(2,1)S(1)} %copy-done.3, ...), custom_call_target="tpu_custom_call" | custom-call | tf_op jit(solution)/shard_map/pallas_call | solution.py:213
  207.4 0.7 reduce_sum.441
  208.0 0.1 reduce_sum.439.refs_1_
  208.1 14.5 %shard_map.105 = (f32[8,31,512]{2,1,0:T(8,128)S(1)}, bf16[4,64,1280]{2,1,0:T(8,128)(2,1)S(1)}) custom-call(f32[31,512]{1,0:T(8,128)S(1)} %reduce_sum.438.refs_0_, bf16[64,1280]{1,0:T(8,128)(2,1)S(1)} %reduce_sum.439.refs_1_), custom_call_target="tpu_custom_call" | custom-call | tf_op jit(solution)/shard_map/pallas_call | solution.py:213
  222.6 0.7 reduce_sum.440
  223.3 1.6 maximum_convert_fusion.2
  225.2 0.3 maximum_convert_fusion.1
  225.4 0.6 copy-done.6
  226.1 0.3 copy-done.10
  226.7 9.5 %fusion.90 = (bf16[1,256,2048]{2,1,0:T(8,128)(2,1)}, bf16[256,2048]{1,0:T(8,128)(2,1)S(1)}) fusion(bf16[1,256,2048]{2,1,0:T(8,128)(2,1)S(1)} %copy-done.10, bf16[1,256,2048]{2,1,0:T(8,128)(2,1)S(1)} %copy-done.6, f32[286,2048]{1,0:T(8,128)S(1)} %maximum_convert_fusion.1, f32[2048]{0:T(1024)S(1)} %bitcast.171, f32[2048]{0:T(1024)S(1)} %bitcast.173, ...), kind=kLoop, calls=%fused_computation.167 | loop fusion | flops 38273024 | bytes 69459968 | tf_op jit(solution)/shard_map/broadcast_in_dim | solution.py:342
  236.2 1.6 fusion.91
  (155 shorter events, 0.5 us)
Async XLA Ops:
  2.1 1.8 copy-start.11
  2.3 3.2 %copy-start.5 = (bf16[1,256,2048]{2,1,0:T(8,128)(2,1)S(1)}, bf16[1,256,2048]{2,1,0:T(8,128)(2,1)}, u32[]{:S(2)}) copy-start(bf16[1,256,2048]{2,1,0:T(8,128)(2,1)} %param.7) | copy-start | bytes 3145732
  2.3 3.2 %copy-start.9 = (bf16[1,256,2048]{2,1,0:T(8,128)(2,1)S(1)}, bf16[1,256,2048]{2,1,0:T(8,128)(2,1)}, u32[]{:S(2)}) copy-start(bf16[1,256,2048]{2,1,0:T(8,128)(2,1)} %param.6) | copy-start | bytes 3145732
  18.0 11.6 %copy-start.40 = (f32[1,4,512]{2,0,1:T(1,128)}, f32[1,4,512]{2,0,1:T(1,128)S(1)}, u32[]{:S(2)}) copy-start(f32[1,4,512]{2,0,1:T(1,128)S(1)} %get-tuple-element.78) | copy-start | bytes 24580
  18.1 11.6 %copy-start.42 = (f32[1,4,512]{2,0,1:T(1,128)}, f32[1,4,512]{2,0,1:T(1,128)S(1)}, u32[]{:S(2)}) copy-start(f32[1,4,512]{2,0,1:T(1,128)S(1)} %get-tuple-element.79) | copy-start | bytes 24580
  18.1 11.6 %copy-start.44 = (f32[1,4,512]{2,0,1:T(1,128)}, f32[1,4,512]{2,0,1:T(1,128)S(1)}, u32[]{:S(2)}) copy-start(f32[1,4,512]{2,0,1:T(1,128)S(1)} %get-tuple-element.80) | copy-start | bytes 24580
  18.1 11.6 %copy-start.46 = (f32[1,4,512]{2,0,1:T(1,128)}, f32[1,4,512]{2,0,1:T(1,128)S(1)}, u32[]{:S(2)}) copy-start(f32[1,4,512]{2,0,1:T(1,128)S(1)} %get-tuple-element.81) | copy-start | bytes 24580
  18.1 11.6 %copy-start.48 = (f32[1,4,512]{2,0,1:T(1,128)}, f32[1,4,512]{2,0,1:T(1,128)S(1)}, u32[]{:S(2)}) copy-start(f32[1,4,512]{2,0,1:T(1,128)S(1)} %get-tuple-element.82) | copy-start | bytes 24580
  18.1 11.6 %copy-start.50 = (f32[1,4,512]{2,0,1:T(1,128)}, f32[1,4,512]{2,0,1:T(1,128)S(1)}, u32[]{:S(2)}) copy-start(f32[1,4,512]{2,0,1:T(1,128)S(1)} %get-tuple-element.83) | copy-start | bytes 24580
  18.1 11.6 %copy-start.52 = (f32[1,4,512]{2,0,1:T(1,128)}, f32[1,4,512]{2,0,1:T(1,128)S(1)}, u32[]{:S(2)}) copy-start(f32[1,4,512]{2,0,1:T(1,128)S(1)} %get-tuple-element.84) | copy-start | bytes 24580
  18.1 11.6 %copy-start.54 = (f32[1,4,512]{2,0,1:T(1,128)}, f32[1,4,512]{2,0,1:T(1,128)S(1)}, u32[]{:S(2)}) copy-start(f32[1,4,512]{2,0,1:T(1,128)S(1)} %get-tuple-element.85) | copy-start | bytes 24580
  18.1 11.6 %copy-start.56 = (f32[1,4,512]{2,0,1:T(1,128)}, f32[1,4,512]{2,0,1:T(1,128)S(1)}, u32[]{:S(2)}) copy-start(f32[1,4,512]{2,0,1:T(1,128)S(1)} %get-tuple-element.86) | copy-start | bytes 24580
  18.1 11.6 %copy-start.58 = (f32[1,4,512]{2,0,1:T(1,128)}, f32[1,4,512]{2,0,1:T(1,128)S(1)}, u32[]{:S(2)}) copy-start(f32[1,4,512]{2,0,1:T(1,128)S(1)} %get-tuple-element.87) | copy-start | bytes 24580
  18.1 11.6 %copy-start.60 = (f32[1,4,512]{2,0,1:T(1,128)}, f32[1,4,512]{2,0,1:T(1,128)S(1)}, u32[]{:S(2)}) copy-start(f32[1,4,512]{2,0,1:T(1,128)S(1)} %get-tuple-element.88) | copy-start | bytes 24580
  18.2 11.6 %copy-start.62 = (f32[1,4,512]{2,0,1:T(1,128)}, f32[1,4,512]{2,0,1:T(1,128)S(1)}, u32[]{:S(2)}) copy-start(f32[1,4,512]{2,0,1:T(1,128)S(1)} %get-tuple-element.89) | copy-start | bytes 24580
  18.2 11.6 %copy-start.64 = (f32[1,4,512]{2,0,1:T(1,128)}, f32[1,4,512]{2,0,1:T(1,128)S(1)}, u32[]{:S(2)}) copy-start(f32[1,4,512]{2,0,1:T(1,128)S(1)} %get-tuple-element.90) | copy-start | bytes 24580
  18.2 11.6 %copy-start.66 = (f32[1,4,512]{2,0,1:T(1,128)}, f32[1,4,512]{2,0,1:T(1,128)S(1)}, u32[]{:S(2)}) copy-start(f32[1,4,512]{2,0,1:T(1,128)S(1)} %get-tuple-element.91) | copy-start | bytes 24580
  18.2 11.6 %copy-start.68 = (f32[1,4,512]{2,0,1:T(1,128)}, f32[1,4,512]{2,0,1:T(1,128)S(1)}, u32[]{:S(2)}) copy-start(f32[1,4,512]{2,0,1:T(1,128)S(1)} %get-tuple-element.92) | copy-start | bytes 24580
  18.2 11.6 %copy-start.70 = (f32[1,4,512]{2,0,1:T(1,128)}, f32[1,4,512]{2,0,1:T(1,128)S(1)}, u32[]{:S(2)}) copy-start(f32[1,4,512]{2,0,1:T(1,128)S(1)} %get-tuple-element.93) | copy-start | bytes 24580
  18.2 11.6 %copy-start.72 = (f32[1,4,512]{2,0,1:T(1,128)}, f32[1,4,512]{2,0,1:T(1,128)S(1)}, u32[]{:S(2)}) copy-start(f32[1,4,512]{2,0,1:T(1,128)S(1)} %get-tuple-element.94) | copy-start | bytes 24580
  18.2 11.6 %copy-start.74 = (f32[1,4,512]{2,0,1:T(1,128)}, f32[1,4,512]{2,0,1:T(1,128)S(1)}, u32[]{:S(2)}) copy-start(f32[1,4,512]{2,0,1:T(1,128)S(1)} %get-tuple-element.95) | copy-start | bytes 24580
  18.2 11.6 %copy-start.76 = (f32[1,4,512]{2,0,1:T(1,128)}, f32[1,4,512]{2,0,1:T(1,128)S(1)}, u32[]{:S(2)}) copy-start(f32[1,4,512]{2,0,1:T(1,128)S(1)} %get-tuple-element.96) | copy-start | bytes 24580
  18.7 11.6 %copy-start.78 = (f32[2048]{0:T(1024)S(1)}, f32[2048]{0:T(1024)}, u32[]{:S(2)}) copy-start(f32[2048]{0:T(1024)} %param.10) | copy-start | bytes 24580
  29.9 2.3 copy-start.15
  32.2 2.4 %copy-start.2 = (bf16[256,2048]{1,0:T(8,128)(2,1)S(1)}, bf16[256,2048]{1,0:T(8,128)(2,1)}, u32[]{:S(2)}) copy-start(bf16[256,2048]{1,0:T(8,128)(2,1)} %param.11) | copy-start | bytes 3145732
  34.6 84.8 %copy-start.16 = (bf16[1,256,2048]{2,1,0:T(8,128)(2,1)S(1)}, bf16[1,256,2048]{2,1,0:T(8,128)(2,1)}, u32[]{:S(2)}) copy-start(bf16[1,256,2048]{2,1,0:T(8,128)(2,1)} %param.8) | copy-start | bytes 3145732
  119.4 8.9 %copy-start = (bf16[1024,1280]{1,0:T(8,128)(2,1)}, bf16[1024,1280]{1,0:T(8,128)(2,1)S(1)}, u32[]{:S(2)}) copy-start(bf16[1024,1280]{1,0:T(8,128)(2,1)S(1)} %get-tuple-element.26) | copy-start | bytes 7864324
  136.2 4.0 %copy-start.7 = (bf16[256,2048]{1,0:T(8,128)(2,1)}, bf16[256,2048]{1,0:T(8,128)(2,1)S(1)}, u32[]{:S(2)}) copy-start(bf16[256,2048]{1,0:T(8,128)(2,1)S(1)} %get-tuple-element.71) | copy-start | bytes 3145732
  140.3 3.1 %copy-start.1 = (bf16[1024,1280]{1,0:T(8,128)(2,1)S(1)}, bf16[1024,1280]{1,0:T(8,128)(2,1)}, u32[]{:S(2)}) copy-start(bf16[1024,1280]{1,0:T(8,128)(2,1)} %copy-done) | copy-start | bytes 7864324
  140.3 3.1 %copy-start.13 = (bf16[256,2048]{1,0:T(8,128)(2,1)S(1)}, bf16[256,2048]{1,0:T(8,128)(2,1)}, u32[]{:S(2)}) copy-start(bf16[256,2048]{1,0:T(8,128)(2,1)} %copy-done.12) | copy-start | bytes 3145732
  140.3 3.1 %copy-start.14 = (bf16[256,4,4,64]{0,3,2,1:T(8,128)(2,1)S(1)}, bf16[256,4,4,64]{0,3,2,1:T(8,128)(2,1)}, u32[]{:S(2)}) copy-start(bf16[256,4,4,64]{0,3,2,1:T(8,128)(2,1)} %copy.21) | copy-start | bytes 1572868
  208.1 16.7 %copy-start.8 = (bf16[256,2048]{1,0:T(8,128)(2,1)S(1)}, bf16[256,2048]{1,0:T(8,128)(2,1)}, u32[]{:S(2)}) copy-start(bf16[256,2048]{1,0:T(8,128)(2,1)} %copy-done.7) | copy-start | bytes 3145732
  208.1 16.7 %copy-start.17 = (bf16[30,2048]{1,0:T(8,128)(2,1)S(1)}, bf16[30,2048]{1,0:T(8,128)(2,1)}, u32[]{:S(2)}) copy-start(bf16[30,2048]{1,0:T(8,128)(2,1)} %slice_select_fusion) | copy-start | bytes 368644
  224.9 1.5 copy-start.10
  224.9 1.5 copy-start.19
  224.9 1.5 copy-start.21
  224.9 1.5 copy-start.23
  224.9 1.5 copy-start.25
  224.9 1.5 copy-start.27
  224.9 1.5 copy-start.29
  224.9 1.5 copy-start.31
  224.9 1.5 copy-start.33
  225.0 1.5 copy-start.35
  225.0 1.5 copy-start.37
  225.0 1.5 copy-start.39
  225.0 1.5 copy-start.41
  225.0 1.5 copy-start.43
  225.0 1.5 copy-start.45
  (31 other events, 36.8 us)
